TPU v7x, 512 devices: a whole 4x8x8 slice. The times are simulated.
512 devices in a mesh: sp: 64 (over z, y), tp: 8 (over x, core).
Axes of the slice: x: 4, y: 8, z: 8, core: 2. Of those that a mesh axis runs over, the one named last changes fastest.
Arguments:
- queries: bfloat16 [1, 24576, 2048], P(None, 'sp', 'tp'), may hold values from -5 to 5
- keys: bfloat16 [1, 24576, 2048], P(None, 'sp', 'tp'), may hold values from -5 to 5
- values: bfloat16 [1, 24576, 2048], P(None, 'sp', 'tp'), may hold values from -6 to 6
- rel_bias: float32 [16, 192], P('tp'), may hold values from -3 to 3
- out_grad: bfloat16 [1, 24576, 2048], P(None, 'sp', 'tp'), may hold values from -48 to 48
Outputs:
- query_grad: bfloat16 [1, 24576, 2048], P(None, 'sp', 'tp')
- key_grad: bfloat16 [1, 24576, 2048], P(None, 'sp', 'tp')
- value_grad: bfloat16 [1, 24576, 2048], P(None, 'sp', 'tp')
- bias_grad: float32 [16, 192], replicated
All inputs are finite; a program needn't handle non-finite values.
Results may differ from a plain program's by a relative error of at most 0.0049.
Values may be sent and summed in bfloat16 or wider, within the bound.
A program may use at most 64 MiB of HBM per device.

v0:
```python
import jax
import jax.numpy as jnp
from jax import lax
from jax.sharding import PartitionSpec as P

HEAD_DIM = 128
SEG = 64
LEFT = 4
CLIP = 128
BAND = 320
BUCKETS = 192


def from_behind(value, axis, steps):
    count = lax.axis_size(axis)
    leading, last = (max(0, -steps), min(count, count - steps))
    return lax.ppermute(value, axis, [(source, source + steps) for source in range(leading, last)])


def copy_for_each(shard, axis):
    copies = jnp.broadcast_to(shard, (lax.axis_size(axis), *shard.shape))
    return lax.all_to_all(copies, axis, split_axis=0, concat_axis=0, tiled=True)


def taken_together(shard, axis):
    everything = copy_for_each(shard, axis)
    return jnp.sum(everything, axis=0)


def joined_along(pieces, dim):
    shape = list(pieces.shape[1:])
    shape[dim] *= pieces.shape[0]
    return jnp.moveaxis(pieces, 0, dim).reshape(shape)


def collect(shard, axis, dim):
    return joined_along(copy_for_each(shard, axis), dim)


def diagonal_onehot():
    span = SEG + BAND - 1
    diag = jnp.arange(span, dtype=jnp.int32)
    bucket = jnp.clip(SEG - 1 - diag + LEFT * SEG, 1 - SEG, CLIP) + SEG - 1
    return (bucket[None, :] == jnp.arange(BUCKETS, dtype=jnp.int32)[:, None]).astype(jnp.float32)


def on_diagonals(rel_bias, onehot):
    return jnp.dot(
        rel_bias, onehot, preferred_element_type=jnp.float32, precision=lax.Precision.HIGHEST
    )


def fill_toeplitz(diag_vals):
    head_count, span = diag_vals.shape
    tiled = jnp.tile(diag_vals, (1, SEG))[:, SEG - 1 :]
    tiled = tiled[:, : SEG * (span - 1)].reshape(head_count, SEG, span - 1)
    return tiled[:, :, :BAND]


def sum_diagonals(terms):
    head_count = terms.shape[0]
    span = SEG + BAND - 1
    padded = jnp.concatenate(
        [
            jnp.zeros((head_count, SEG, SEG - 1), jnp.float32),
            terms,
            jnp.zeros((head_count, SEG, SEG), jnp.float32),
        ],
        axis=2,
    )
    width = padded.shape[2]
    flat = jnp.concatenate(
        [padded.reshape(head_count, SEG * width), jnp.zeros((head_count, SEG), jnp.float32)], axis=1
    )
    skewed = flat.reshape(head_count, SEG, width + 1)[:, :, :span]
    return jnp.sum(skewed, axis=1)


def band_core(q_segs, k_band, v_band, g_segs, table, key_valid):
    seg_count = q_segs.shape[1]
    score_scale = HEAD_DIM ** (-0.5)
    score_parts = []
    prob_parts = []
    for offset in range(LEFT + 1):
        score_parts.append(
            jnp.einsum(
                "sncha,snkha->snhck",
                q_segs,
                k_band[:, offset : offset + seg_count],
                preferred_element_type=jnp.float32,
            )
        )
        prob_parts.append(
            jnp.einsum(
                "sncha,snkha->snhck",
                g_segs,
                v_band[:, offset : offset + seg_count],
                preferred_element_type=jnp.float32,
            )
        )
    score = jnp.concatenate(score_parts, axis=-1) * score_scale + table[None, None]
    score = jnp.where(key_valid[None, :, None, None, :], score, -jnp.inf)
    row_max = jnp.max(score, axis=-1, keepdims=True)
    expo = jnp.exp(score - row_max)
    row_sum = jnp.sum(expo, axis=-1, keepdims=True)
    prob = expo / row_sum
    log_norm = (row_max + jnp.log(row_sum))[..., 0]
    prob_grad = jnp.concatenate(prob_parts, axis=-1)
    row_delta = jnp.sum(prob * prob_grad, axis=-1)
    score_grad = prob * (prob_grad - row_delta[..., None])
    bias_terms = jnp.sum(score_grad, axis=(0, 1))
    prob_low = prob.astype(jnp.bfloat16)
    grad_low = (score_grad * score_scale).astype(jnp.bfloat16)
    query_acc = jnp.zeros(q_segs.shape, jnp.float32)
    key_acc = jnp.zeros(k_band.shape, jnp.float32)
    value_acc = jnp.zeros(k_band.shape, jnp.float32)
    for offset in range(LEFT + 1):
        grad_part = grad_low[..., offset * SEG : (offset + 1) * SEG]
        prob_part = prob_low[..., offset * SEG : (offset + 1) * SEG]
        query_acc = query_acc + jnp.einsum(
            "snhck,snkha->sncha",
            grad_part,
            k_band[:, offset : offset + seg_count],
            preferred_element_type=jnp.float32,
        )
        first_seg = 0
        key_acc = key_acc.at[:, offset + first_seg : offset + seg_count].add(
            jnp.einsum("snhck,sncha->snkha", grad_part, q_segs, preferred_element_type=jnp.float32)
        )
        value_acc = value_acc.at[:, offset + first_seg : offset + seg_count].add(
            jnp.einsum("snhck,sncha->snkha", prob_part, g_segs, preferred_element_type=jnp.float32)
        )
    return (query_acc, key_acc, value_acc, bias_terms, log_norm, row_delta)


def local(queries, keys, values, rel_bias, out_grad):
    seq_count, tok_rows, row_width = queries.shape
    head_count = row_width // HEAD_DIM
    seg_count = tok_rows // SEG
    reach = LEFT * SEG
    seq_index = lax.axis_index("sp")
    seg_shape = (seq_count, seg_count, SEG, head_count, HEAD_DIM)
    band_shape = (seq_count, seg_count + LEFT, SEG, head_count, HEAD_DIM)
    onehot = diagonal_onehot()
    table = fill_toeplitz(on_diagonals(rel_bias, onehot))
    prior_k, prior_v = from_behind(
        (keys[:, tok_rows - reach :], values[:, tok_rows - reach :]), "sp", 1
    )
    k_band = jnp.concatenate([prior_k, keys], axis=1).reshape(band_shape)
    v_band = jnp.concatenate([prior_v, values], axis=1).reshape(band_shape)
    q_segs = queries.reshape(seg_shape)
    g_segs = out_grad.reshape(seg_shape)
    positions = (
        seq_index * tok_rows
        + jnp.arange(seg_count, dtype=jnp.int32)[:, None] * SEG
        - reach
        + jnp.arange(BAND, dtype=jnp.int32)[None, :]
    )
    key_valid = positions >= 0
    flat = (seq_count, reach + tok_rows, row_width)
    query_acc, key_acc, value_acc, bias_terms, log_norm, row_delta = band_core(
        q_segs, k_band, v_band, g_segs, table, key_valid
    )
    key_flat = key_acc.reshape(flat)
    value_flat = value_acc.reshape(flat)
    back_k, back_v = from_behind((key_flat[:, :reach], value_flat[:, :reach]), "sp", -1)
    key_own = key_flat[:, reach:].at[:, tok_rows - reach :].add(back_k)
    value_own = value_flat[:, reach:].at[:, tok_rows - reach :].add(back_v)
    query_grad = query_acc.astype(jnp.bfloat16).reshape(seq_count, tok_rows, row_width)
    key_grad = key_own.astype(jnp.bfloat16)
    value_grad = value_own.astype(jnp.bfloat16)
    local_bias = jnp.dot(
        sum_diagonals(bias_terms),
        onehot.T,
        preferred_element_type=jnp.float32,
        precision=lax.Precision.HIGHEST,
    )
    summed = taken_together(local_bias, "sp")
    bias_grad = collect(summed, "tp", 0)
    return (query_grad, key_grad, value_grad, bias_grad)


def solution(mesh):
    return jax.shard_map(
        local,
        mesh=mesh,
        in_specs=(
            P(None, "sp", "tp"),
            P(None, "sp", "tp"),
            P(None, "sp", "tp"),
            P("tp", None),
            P(None, "sp", "tp"),
        ),
        out_specs=(P(None, "sp", "tp"), P(None, "sp", "tp"), P(None, "sp", "tp"), P()),
        check_vma=False,
    )
```

profile of v0, /device:TPU:1, one launch (start us, length us, event | category | flops | bytes accessed | tf_op | source)
XLA Modules:
  0.0 84.2 jit_solution(5421645292207113864)
XLA Ops:
  0.6 0.9 %slice.478 = bf16[1,256,256]{2,1,0:T(8,128)(2,1)S(1)} slice(bf16[1,384,256]{2,1,0:T(8,128)(2,1)} %param.30), slice={[0:1], [128:384], [0:256]} | slice | bytes 262144 | tf_op jit(solution)/shard_map/slice | solution.py:147
  1.6 4.0 %collective-permute-start = (bf16[1,256,256]{2,1,0:T(8,128)(2,1)S(1)}, bf16[1,256,256]{2,1,0:T(8,128)(2,1)S(1)}, u32[]{:S(2)}, u32[]{:S(2)}) collective-permute-start(bf16[1,256,256]{2,1,0:T(8,128)(2,1)S(1)} %slice.478), channel_id=1, source_target_pairs={{0,8},{8,16},{16,24},{24,32},{32,40},{40,48},{48,56},{56,64},{64,7... | collective-permute-start | bytes 393224 | tf_op jit(solution)/shard_map/ppermute | solution.py:17
  5.6 0.9 %slice.486 = bf16[1,256,256]{2,1,0:T(8,128)(2,1)S(1)} slice(bf16[1,384,256]{2,1,0:T(8,128)(2,1)} %param.31), slice={[0:1], [128:384], [0:256]} | slice | bytes 262144 | tf_op jit(solution)/shard_map/slice | solution.py:147
  6.5 3.3 %collective-permute-start.1 = (bf16[1,256,256]{2,1,0:T(8,128)(2,1)S(1)}, bf16[1,256,256]{2,1,0:T(8,128)(2,1)S(1)}, u32[]{:S(2)}, u32[]{:S(2)}) collective-permute-start(bf16[1,256,256]{2,1,0:T(8,128)(2,1)S(1)} %slice.486), channel_id=1, source_target_pairs={{0,8},{8,16},{16,24},{24,32},{32,40},{40,48},{48,56},{56,64},{64,7... | collective-permute-start | bytes 393224 | tf_op jit(solution)/shard_map/ppermute | solution.py:17
  9.9 1.0 %reshape.1130 = bf16[6,64,2,128]{3,2,1,0:T(2,128)(2,1)S(1)} reshape(bf16[1,384,256]{2,1,0:T(8,128)(2,1)} %param.33) | data formatting | bytes 393216 | tf_op jit(solution)/shard_map/reshape.447
  10.9 1.0 %reshape.1122 = bf16[6,64,2,128]{3,2,1,0:T(2,128)(2,1)S(1)} reshape(bf16[1,384,256]{2,1,0:T(8,128)(2,1)} %param.29) | data formatting | bytes 393216 | tf_op jit(solution)/shard_map/reshape.428
  16.7 1.0 %convolution_bitcast_fusion.13 = f32[1,6,2,64,64]{4,3,2,1,0:T(8,128)} fusion(bf16[1,6,64,2,128]{4,3,2,1,0:T(2,128)(2,1)S(1)} %get-tuple-element.171, bf16[6,64,2,128]{3,2,1,0:T(2,128)(2,1)S(1)} %reshape.1130), kind=kOutput, calls=%fused_computation.17 | convolution fusion | flops 12582912 | bytes 589824 | tf_op jit(solution)/shard_map/sncha,snkha->snhck/dot_general | solution.py:94
  17.7 1.0 %convolution_bitcast_fusion.12 = f32[1,6,2,64,64]{4,3,2,1,0:T(8,128)} fusion(bf16[1,6,64,2,128]{4,3,2,1,0:T(2,128)(2,1)S(1)} %get-tuple-element.170, bf16[6,64,2,128]{3,2,1,0:T(2,128)(2,1)S(1)} %reshape.1130), kind=kOutput, calls=%fused_computation.16 | convolution fusion | flops 12582912 | bytes 589824 | tf_op jit(solution)/shard_map/sncha,snkha->snhck/dot_general | solution.py:94
  18.7 1.0 %convolution_bitcast_fusion.11 = f32[1,6,2,64,64]{4,3,2,1,0:T(8,128)} fusion(bf16[1,6,64,2,128]{4,3,2,1,0:T(2,128)(2,1)S(1)} %get-tuple-element.169, bf16[6,64,2,128]{3,2,1,0:T(2,128)(2,1)S(1)} %reshape.1130), kind=kOutput, calls=%fused_computation.15 | convolution fusion | flops 12582912 | bytes 589824 | tf_op jit(solution)/shard_map/sncha,snkha->snhck/dot_general | solution.py:94
  19.6 1.0 %convolution_bitcast_fusion.10 = f32[1,6,2,64,64]{4,3,2,1,0:T(8,128)} fusion(bf16[1,6,64,2,128]{4,3,2,1,0:T(2,128)(2,1)S(1)} %get-tuple-element.168, bf16[6,64,2,128]{3,2,1,0:T(2,128)(2,1)S(1)} %reshape.1130), kind=kOutput, calls=%fused_computation.14 | convolution fusion | flops 12582912 | bytes 589824 | tf_op jit(solution)/shard_map/sncha,snkha->snhck/dot_general | solution.py:94
  21.3 1.0 %convolution_bitcast_fusion.16 = f32[1,6,2,64,64]{4,3,2,1,0:T(8,128)} fusion(bf16[1,6,64,2,128]{4,3,2,1,0:T(2,128)(2,1)S(1)} %get-tuple-element.164, bf16[6,64,2,128]{3,2,1,0:T(2,128)(2,1)S(1)} %reshape.1122), kind=kOutput, calls=%fused_computation.20 | convolution fusion | flops 12582912 | bytes 589824 | tf_op jit(solution)/shard_map/sncha,snkha->snhck/dot_general | solution.py:86
  22.3 1.0 %convolution_bitcast_fusion.15 = f32[1,6,2,64,64]{4,3,2,1,0:T(8,128)} fusion(bf16[1,6,64,2,128]{4,3,2,1,0:T(2,128)(2,1)S(1)} %get-tuple-element.163, bf16[6,64,2,128]{3,2,1,0:T(2,128)(2,1)S(1)} %reshape.1122), kind=kOutput, calls=%fused_computation.19 | convolution fusion | flops 12582912 | bytes 589824 | tf_op jit(solution)/shard_map/sncha,snkha->snhck/dot_general | solution.py:86
  23.3 1.5 %concatenate.116 = f32[1,6,2,64,320]{4,3,2,1,0:T(8,128)S(1)} concatenate(f32[1,6,2,64,64]{4,3,2,1,0:T(8,128)S(1)} %convolution_bitcast_fusion.19, f32[1,6,2,64,64]{4,3,2,1,0:T(8,128)S(1)} %convolution_bitcast_fusion.18, f32[1,6,2,64,64]{4,3,2,1,0:T(8,128)S(1)} %convolution_bitcast_fusion.17, f32[1,6,2,64,64]{4,3,2,1,0:T(8,128)} %convolution_bitcast_fusion.16, ...), dimensions={4} | concatenate | bytes 1966080 | tf_op jit(solution)/shard_map/concatenate | solution.py:101
  25.6 1.7 %concatenate.123 = f32[1,6,2,64,320]{4,3,2,1,0:T(8,128)S(1)} concatenate(f32[1,6,2,64,64]{4,3,2,1,0:T(8,128)S(1)} %convolution_bitcast_fusion.14, f32[1,6,2,64,64]{4,3,2,1,0:T(8,128)} %convolution_bitcast_fusion.13, f32[1,6,2,64,64]{4,3,2,1,0:T(8,128)} %convolution_bitcast_fusion.12, f32[1,6,2,64,64]{4,3,2,1,0:T(8,128)} %convolution_bitcast_fusion.11, ...), dimensions={4} | concatenate | bytes 1966080 | tf_op jit(solution)/shard_map/concatenate | solution.py:108
  27.9 1.4 %fusion.21 = (f32[2,64,320]{2,1,0:T(8,128)S(1)}, bf16[1,6,2,64,320]{4,3,2,1,0:T(8,128)(2,1)S(1)}, bf16[1,6,2,64,320]{4,3,2,1,0:T(8,128)(2,1)S(1)}) fusion(f32[1,6,2,64,320]{4,3,2,1,0:T(8,128)S(1)} %concatenate.123, f32[6,2,64]{2,1,0:T(2,128)S(1)} %multiply_reduce_fusion, f32[6,2,64]{2,1,0:T(2,128)} %copy-done.14, f32[6,2,64]{2,1,0:T(2,128)S(1)} %fusion.20, ...), kind=kLoop, calls=%fused_computation.51 | loop fusion | flops 2662400 | bytes 3287936 | tf_op jit(solution)/shard_map/reduce_sum | solution.py:111
  33.5 0.9 %slice.539 = f32[1,256,256]{2,0,1:T(1,128)} slice(f32[1,640,256]{2,0,1:T(1,128)S(1)} %bitcast.217), slice={[0:1], [0:256], [0:256]} | slice | bytes 524288 | tf_op jit(solution)/shard_map/slice | solution.py:166
  34.4 1.3 %collective-permute-start.2 = (f32[1,256,256]{2,0,1:T(1,128)}, f32[1,256,256]{2,0,1:T(1,128)}, u32[]{:S(2)}, u32[]{:S(2)}) collective-permute-start(f32[1,256,256]{2,0,1:T(1,128)} %slice.539), channel_id=1, source_target_pairs={{8,0},{16,8},{24,16},{32,24},{40,32},{48,40},{56,48},{64,56},{72,6... | collective-permute-start | bytes 786440 | tf_op jit(solution)/shard_map/ppermute | solution.py:17
  38.9 17.6 %all-to-all-start = ((f32[64,2,192]{2,1,0:T(2,128)}), f32[64,2,192]{2,1,0:T(2,128)S(1)}, u32[]{:S(2)}, u32[]{:S(2)}) async-start(f32[64,2,192]{2,1,0:T(2,128)} %broadcast_in_dim.38), calls=%async_computation | async-start | bytes 262144 | tf_op jit(solution)/shard_map/all_to_all | solution.py:22
  56.5 1.2 %fusion.15 = f32[1,10,64,2,128]{4,2,3,1,0:T(8,128)S(1)} fusion(f32[1,10,64,2,128]{4,2,3,1,0:T(8,128)S(1)} %fusion.13, bf16[1,6,2,64,320]{4,3,2,1,0:T(8,128)(2,1)} %copy-done.1, bf16[6,64,2,128]{3,2,1,0:T(2,128)(2,1)S(1)} %reshape.1130), kind=kOutput, calls=%fused_computation.39 | convolution fusion | flops 12681216 | bytes 1179648 | tf_op jit(solution)/shard_map/snhck,sncha->snkha/dot_general | solution.py:131
  59.2 1.3 %collective-permute-start.3 = (f32[1,256,256]{2,0,1:T(1,128)}, f32[1,256,256]{2,0,1:T(1,128)S(1)}, u32[]{:S(2)}, u32[]{:S(2)}) collective-permute-start(f32[1,256,256]{2,0,1:T(1,128)} %slice.550), channel_id=1, source_target_pairs={{8,0},{16,8},{24,16},{32,24},{40,32},{48,40},{56,48},{64,56},{72,6... | collective-permute-start | bytes 786440 | tf_op jit(solution)/shard_map/ppermute | solution.py:17
  60.4 7.5 %all-to-all-done = f32[64,2,192]{2,1,0:T(2,128)S(1)} async-done(((f32[64,2,192]{2,1,0:T(2,128)}), f32[64,2,192]{2,1,0:T(2,128)S(1)}, u32[]{:S(2)}, u32[]{:S(2)}) %all-to-all-start) | async-done | bytes 98336 | tf_op jit(solution)/shard_map/all_to_all | solution.py:22
  68.6 7.3 %all-to-all-start.1 = ((f32[8,2,192]{2,1,0:T(2,128)}), f32[8,2,192]{2,1,0:T(2,128)S(1)}, u32[]{:S(2)}, u32[]{:S(2)}) async-start(f32[8,2,192]{2,1,0:T(2,128)} %broadcast_in_dim.39), calls=%async_computation.1 | async-start | bytes 32768 | tf_op jit(solution)/shard_map/all_to_all | solution.py:22
  77.7 2.9 %all-to-all-done.1 = f32[8,2,192]{2,1,0:T(2,128)S(1)} async-done(((f32[8,2,192]{2,1,0:T(2,128)}), f32[8,2,192]{2,1,0:T(2,128)S(1)}, u32[]{:S(2)}, u32[]{:S(2)}) %all-to-all-start.1) | async-done | bytes 12320 | tf_op jit(solution)/shard_map/all_to_all | solution.py:22
  81.2 1.3 %fusion.24 = bf16[1,384,256]{2,0,1:T(2,128)(2,1)S(1)} fusion(bf16[1,384,256]{2,0,1:T(2,128)(2,1)S(1)} %slice.537, f32[1,256,256]{2,0,1:T(1,128)} %collective-permute-done.2, f32[1,640,256]{2,0,1:T(1,128)S(1)} %bitcast.219), kind=kLoop, calls=%fused_computation.59 | loop fusion | flops 65536 | bytes 786432 | tf_op jit(solution)/shard_map/scatter-add | solution.py:167
  (103 shorter events, 20.1 us)
Async XLA Ops:
  0.6 11.2 %copy-start = (f32[2,192]{1,0:T(2,128)S(1)}, f32[2,192]{1,0:T(2,128)}, u32[]{:S(2)}) copy-start(f32[2,192]{1,0:T(2,128)} %param.32) | copy-start | bytes 4612
  1.6 12.8 %collective-permute-start = (bf16[1,256,256]{2,1,0:T(8,128)(2,1)S(1)}, bf16[1,256,256]{2,1,0:T(8,128)(2,1)S(1)}, u32[]{:S(2)}, u32[]{:S(2)}) collective-permute-start(bf16[1,256,256]{2,1,0:T(8,128)(2,1)S(1)} %slice.478), channel_id=1, source_target_pairs={{0,8},{8,16},{16,24},{24,32},{32,40},{40,48},{48,56},{56,64},{64,7... | collective-permute-start | bytes 393224 | tf_op jit(solution)/shard_map/ppermute | solution.py:17
  6.5 7.9 %copy-start.12 = (bf16[1,384,256]{2,1,0:T(8,128)(2,1)S(1)}, bf16[1,384,256]{2,1,0:T(8,128)(2,1)}, u32[]{:S(2)}) copy-start(bf16[1,384,256]{2,1,0:T(8,128)(2,1)} %param.30) | copy-start | bytes 589828
  6.5 8.9 %collective-permute-start.1 = (bf16[1,256,256]{2,1,0:T(8,128)(2,1)S(1)}, bf16[1,256,256]{2,1,0:T(8,128)(2,1)S(1)}, u32[]{:S(2)}, u32[]{:S(2)}) collective-permute-start(bf16[1,256,256]{2,1,0:T(8,128)(2,1)S(1)} %slice.486), channel_id=1, source_target_pairs={{0,8},{8,16},{16,24},{24,32},{32,40},{40,48},{48,56},{56,64},{64,7... | collective-permute-start | bytes 393224 | tf_op jit(solution)/shard_map/ppermute | solution.py:17
  9.9 4.5 %copy-start.17 = (s32[383]{0:T(512)}, s32[383]{0:T(512)S(1)}, u32[]{:S(2)}) copy-start(s32[383]{0:T(512)S(1)} %clamp_add_fusion) | copy-start | bytes 4600
  14.4 1.0 %copy-start.13 = (bf16[1,384,256]{2,1,0:T(8,128)(2,1)S(1)}, bf16[1,384,256]{2,1,0:T(8,128)(2,1)}, u32[]{:S(2)}) copy-start(bf16[1,384,256]{2,1,0:T(8,128)(2,1)} %param.31) | copy-start | bytes 589828
  15.4 5.2 %copy-start.8 = (bf16[1,6,64,2,128]{4,3,2,1,0:T(2,128)(2,1)}, bf16[1,6,64,2,128]{4,3,2,1,0:T(2,128)(2,1)S(1)}, u32[]{:S(2)}) copy-start(bf16[1,6,64,2,128]{4,3,2,1,0:T(2,128)(2,1)S(1)} %get-tuple-element.167) | copy-start | bytes 589828
  15.4 5.5 %copy-start.6 = (bf16[1,6,64,2,128]{4,3,2,1,0:T(2,128)(2,1)}, bf16[1,6,64,2,128]{4,3,2,1,0:T(2,128)(2,1)S(1)}, u32[]{:S(2)}) copy-start(bf16[1,6,64,2,128]{4,3,2,1,0:T(2,128)(2,1)S(1)} %get-tuple-element.166) | copy-start | bytes 589828
  15.4 5.7 %copy-start.4 = (bf16[1,6,64,2,128]{4,3,2,1,0:T(2,128)(2,1)}, bf16[1,6,64,2,128]{4,3,2,1,0:T(2,128)(2,1)S(1)}, u32[]{:S(2)}) copy-start(bf16[1,6,64,2,128]{4,3,2,1,0:T(2,128)(2,1)S(1)} %get-tuple-element.165) | copy-start | bytes 589828
  15.4 5.9 %copy-start.2 = (bf16[1,6,64,2,128]{4,3,2,1,0:T(2,128)(2,1)}, bf16[1,6,64,2,128]{4,3,2,1,0:T(2,128)(2,1)S(1)}, u32[]{:S(2)}) copy-start(bf16[1,6,64,2,128]{4,3,2,1,0:T(2,128)(2,1)S(1)} %get-tuple-element.164) | copy-start | bytes 589828
  15.4 6.9 %copy-start.10 = (bf16[1,6,64,2,128]{4,3,2,1,0:T(2,128)(2,1)}, bf16[1,6,64,2,128]{4,3,2,1,0:T(2,128)(2,1)S(1)}, u32[]{:S(2)}) copy-start(bf16[1,6,64,2,128]{4,3,2,1,0:T(2,128)(2,1)S(1)} %get-tuple-element.163) | copy-start | bytes 589828
  25.5 1.7 %copy-start.14 = (f32[6,2,64]{2,1,0:T(2,128)}, f32[6,2,64]{2,1,0:T(2,128)S(1)}, u32[]{:S(2)}) copy-start(f32[6,2,64]{2,1,0:T(2,128)S(1)} %fusion.19) | copy-start | bytes 9220
  27.9 1.4 %copy-start.9 = (bf16[1,6,64,2,128]{4,3,2,1,0:T(2,128)(2,1)S(1)}, bf16[1,6,64,2,128]{4,3,2,1,0:T(2,128)(2,1)}, u32[]{:S(2)}) copy-start(bf16[1,6,64,2,128]{4,3,2,1,0:T(2,128)(2,1)} %copy-done.8) | copy-start | bytes 589828
  29.3 7.4 %copy-start.1 = (bf16[1,6,2,64,320]{4,3,2,1,0:T(8,128)(2,1)}, bf16[1,6,2,64,320]{4,3,2,1,0:T(8,128)(2,1)S(1)}, u32[]{:S(2)}) copy-start(bf16[1,6,2,64,320]{4,3,2,1,0:T(8,128)(2,1)S(1)} %get-tuple-element.162) | copy-start | bytes 1474564
  29.3 1.1 %copy-start.7 = (bf16[1,6,64,2,128]{4,3,2,1,0:T(2,128)(2,1)S(1)}, bf16[1,6,64,2,128]{4,3,2,1,0:T(2,128)(2,1)}, u32[]{:S(2)}) copy-start(bf16[1,6,64,2,128]{4,3,2,1,0:T(2,128)(2,1)} %copy-done.6) | copy-start | bytes 589828
  29.5 1.2 %copy-start.5 = (bf16[1,6,64,2,128]{4,3,2,1,0:T(2,128)(2,1)S(1)}, bf16[1,6,64,2,128]{4,3,2,1,0:T(2,128)(2,1)}, u32[]{:S(2)}) copy-start(bf16[1,6,64,2,128]{4,3,2,1,0:T(2,128)(2,1)} %copy-done.4) | copy-start | bytes 589828
  30.4 0.9 %copy-start.3 = (bf16[1,6,64,2,128]{4,3,2,1,0:T(2,128)(2,1)S(1)}, bf16[1,6,64,2,128]{4,3,2,1,0:T(2,128)(2,1)}, u32[]{:S(2)}) copy-start(bf16[1,6,64,2,128]{4,3,2,1,0:T(2,128)(2,1)} %copy-done.2) | copy-start | bytes 589828
  34.4 46.7 %collective-permute-start.2 = (f32[1,256,256]{2,0,1:T(1,128)}, f32[1,256,256]{2,0,1:T(1,128)}, u32[]{:S(2)}, u32[]{:S(2)}) collective-permute-start(f32[1,256,256]{2,0,1:T(1,128)} %slice.539), channel_id=1, source_target_pairs={{8,0},{16,8},{24,16},{32,24},{40,32},{48,40},{56,48},{64,56},{72,6... | collective-permute-start | bytes 786440 | tf_op jit(solution)/shard_map/ppermute | solution.py:17
  36.4 0.7 copy-start.15
  37.1 0.9 %copy-start.18 = (s32[383]{0:T(512)S(1)}, s32[383]{0:T(512)}, u32[]{:S(2)}) copy-start(s32[383]{0:T(512)} %copy-done.17) | copy-start | bytes 4600
  38.9 29.0 %all-to-all-start = ((f32[64,2,192]{2,1,0:T(2,128)}), f32[64,2,192]{2,1,0:T(2,128)S(1)}, u32[]{:S(2)}, u32[]{:S(2)}) async-start(f32[64,2,192]{2,1,0:T(2,128)} %broadcast_in_dim.38), calls=%async_computation | async-start | bytes 262144 | tf_op jit(solution)/shard_map/all_to_all | solution.py:22
  57.7 18.1 %copy-start.11 = (bf16[1,6,64,2,128]{4,3,2,1,0:T(2,128)(2,1)S(1)}, bf16[1,6,64,2,128]{4,3,2,1,0:T(2,128)(2,1)}, u32[]{:S(2)}) copy-start(bf16[1,6,64,2,128]{4,3,2,1,0:T(2,128)(2,1)} %copy-done.10) | copy-start | bytes 589828
  59.2 24.0 %collective-permute-start.3 = (f32[1,256,256]{2,0,1:T(1,128)}, f32[1,256,256]{2,0,1:T(1,128)S(1)}, u32[]{:S(2)}, u32[]{:S(2)}) collective-permute-start(f32[1,256,256]{2,0,1:T(1,128)} %slice.550), channel_id=1, source_target_pairs={{8,0},{16,8},{24,16},{32,24},{40,32},{48,40},{56,48},{64,56},{72,6... | collective-permute-start | bytes 786440 | tf_op jit(solution)/shard_map/ppermute | solution.py:17
  68.6 11.9 %all-to-all-start.1 = ((f32[8,2,192]{2,1,0:T(2,128)}), f32[8,2,192]{2,1,0:T(2,128)S(1)}, u32[]{:S(2)}, u32[]{:S(2)}) async-start(f32[8,2,192]{2,1,0:T(2,128)} %broadcast_in_dim.39), calls=%async_computation.1 | async-start | bytes 32768 | tf_op jit(solution)/shard_map/all_to_all | solution.py:22
  (1 other events, 0.7 us)
where the time goes:
time: 84.8 us; the launch traced here: 84.2 us
  starting transfers between devices  34.8 us (41%)
  local copies, waits for them, and re-layouts  20.8 us (25%)
  matrix products  12.3 us (15%)
  waiting for transfers between devices  10.3 us (12%)
  other arithmetic  4.67 us (6%)
  between operations  1.29 us (2%)
    all_to_all x2, starting transfers between devices, copy_for_each(): return lax.all_to_all(copies, axis, split_axis=0, concat_axis=0, tiled=True)  24.8 us
    all_to_all x2, waiting for transfers between devices, copy_for_each(): return lax.all_to_all(copies, axis, split_axis=0, concat_axis=0, tiled=True)  10.3 us
    ppermute x4, starting transfers between devices, from_behind(): lax.ppermute(value, axis, [(source, source + steps) for source in range(l...  9.92 us
    dot_general x5, matrix products, band_core(): jnp.einsum('sncha,snkha->snhck', g_segs, v_band[:, offset:offset + seg_co...  4.16 us
    unnamed x40, local copies, waits for them, and re-layouts  2.63 us
    dot_general x5, matrix products, band_core(): jnp.einsum('sncha,snkha->snhck', q_segs, k_band[:, offset:offset + seg_co...  2.6 us
    dot_general x5, matrix products, band_core(): jnp.einsum('snhck,sncha->snkha', prob_part, g_segs, preferred_element_typ...  2.47 us
    another operation x2, local copies, waits for them, and re-layouts  1.96 us
  transfers between devices with their start and end apart: 6, of which 2 were waited for; matrix products, arithmetic and copies ran while one was open for 20% of the time, Pallas kernels for 0%

commit v1 on v0

v1 whole, which is shorter than its diff:
```python
import functools

import jax
import jax.numpy as jnp
from jax import lax
from jax.experimental import pallas as pl
from jax.experimental.pallas import tpu as pltpu
from jax.sharding import PartitionSpec as P

HEAD_DIM = 128
SEG = 64
LEFT = 4
BUCKETS = 192
HALO = LEFT * SEG
PAIR = 2 * SEG
SPAN = 3 * PAIR
NEG = -1e30
LOG2E = 1.4426950408889634
MESH = pl.DeviceIdType.MESH
F32 = jnp.float32
BF16 = jnp.bfloat16
RING = 8


def dot(a, b, contract):
    return lax.dot_general(a, b, (contract, ((), ())), preferred_element_type=F32)


def lanes_of(head):
    return slice(head * HEAD_DIM, (head + 1) * HEAD_DIM)


def diagonal_sums(block):
    x = jnp.concatenate([block, jnp.zeros_like(block)], axis=1)
    rows = x.shape[0]
    while rows > 1:
        rows //= 2
        x = x[:rows] + pltpu.roll(x[rows:], 2 * PAIR - rows, 1)
    return x


def body(
    tokens, heads, q_hbm, k_hbm, v_hbm, rb_ref, g_hbm,
    dq_ref, dk_ref, dv_ref, db_ref,
    q, g, kb, vb, pt, st, tab, acc, rbs,
    out_k, out_v, in_k, in_v, by, bz, bt,
    load_sem, halo_send, halo_recv, back_send, back_recv,
    y_send, y_recv, z_send, z_recv, t_send, t_recv,
):
    sp = lax.axis_index("sp")
    tp = lax.axis_index("tp")
    ring = lax.axis_size("sp")
    tps = lax.axis_size("tp")
    zs = ring // RING
    yi = lax.rem(sp, RING)
    zi = lax.div(sp, RING)
    nxt = lax.rem(sp + 1, ring)
    prv = lax.rem(sp + ring - 1, ring)
    pairs = tokens // PAIR

    tail = tokens - HALO
    loads = []

    def load(src, dst):
        cp = pltpu.make_async_copy(src, dst, load_sem.at[len(loads)])
        cp.start()
        loads.append(cp)
        return cp

    k_tail = load(k_hbm.at[0, pl.ds(tail, HALO)], kb.at[pl.ds(HALO + tail, HALO)])
    v_tail = load(v_hbm.at[0, pl.ds(tail, HALO)], vb.at[pl.ds(HALO + tail, HALO)])
    k_head = load(k_hbm.at[0, pl.ds(0, tail)], kb.at[pl.ds(HALO, tail)])
    v_head = load(v_hbm.at[0, pl.ds(0, tail)], vb.at[pl.ds(HALO, tail)])
    q_all = load(q_hbm.at[0], q)
    g_all = load(g_hbm.at[0], g)

    y_peers = [zi * RING + lax.rem(yi + i, RING) for i in range(1, RING)]
    z_peers = [lax.rem(zi + i, zs) * RING + yi for i in range(1, zs)]
    t_peers = [lax.rem(tp + i, tps) for i in range(1, tps)]
    barrier = pltpu.get_barrier_semaphore()
    for peer in [nxt, prv] + y_peers + z_peers:
        pl.semaphore_signal(barrier, inc=1, device_id={"sp": peer}, device_id_type=MESH)
    for peer in t_peers:
        pl.semaphore_signal(barrier, inc=1, device_id={"tp": peer}, device_id_type=MESH)
    pl.semaphore_wait(barrier, 2 + len(y_peers) + len(z_peers) + len(t_peers))

    sent = []

    def send(src, dst, ssem, rsem, where):
        cp = pltpu.make_async_remote_copy(
            src_ref=src, dst_ref=dst, send_sem=ssem, recv_sem=rsem,
            device_id=where, device_id_type=MESH,
        )
        cp.start()
        sent.append(cp)
        return cp

    k_tail.wait()
    v_tail.wait()
    halo = {}
    for h in range(heads):
        for part in (1, 0):
            for a, band in enumerate((kb, vb)):
                n = len(halo)
                halo[h, a, part] = send(
                    band.at[pl.ds(tokens + part * PAIR, PAIR), pl.ds(h * HEAD_DIM, HEAD_DIM)],
                    band.at[pl.ds(part * PAIR, PAIR), pl.ds(h * HEAD_DIM, HEAD_DIM)],
                    halo_send.at[n], halo_recv.at[n], {"sp": nxt},
                )

    scale = HEAD_DIM ** (-0.5)
    neg = jnp.where(sp == 0, F32(NEG), F32(0.0))
    rbs[...] = jnp.zeros_like(rbs)
    rbs[0:heads, 0:BUCKETS] = rb_ref[...] * LOG2E
    lane = lax.broadcasted_iota(jnp.int32, (1, 2 * PAIR), 1)
    key_row = lax.broadcasted_iota(jnp.int32, (PAIR, PAIR), 0)
    q_col = lax.broadcasted_iota(jnp.int32, (PAIR, PAIR), 1)
    for h in range(heads):
        row = rbs[h : h + 1, :]
        last = rbs[h : h + 1, BUCKETS - 1 : BUCKETS]
        near = jnp.where(lane < BUCKETS, row, last)
        far = jnp.where((lane >= SEG) & (lane < BUCKETS), row, last)
        shape = (PAIR, 2 * PAIR)
        near = pltpu.roll(jnp.broadcast_to(near, shape), 193, 1, stride=1, stride_axis=0)[:, :PAIR]
        far = pltpu.roll(jnp.broadcast_to(far, shape), 65, 1, stride=1, stride_axis=0)[:, :PAIR]
        tab[h, 0:PAIR] = jnp.where((key_row < SEG) & (q_col >= SEG), NEG, last)
        tab[h, PAIR : 2 * PAIR] = far
        tab[h, 2 * PAIR : SPAN] = jnp.where((key_row >= SEG) & (q_col < SEG), NEG, near)

    for cp in (k_head, v_head, q_all, g_all):
        cp.wait()

    def block(h, p, first):
        ls = lanes_of(h)
        rows = slice(p * PAIR, p * PAIR + SPAN)
        cols = slice(p * PAIR, (p + 1) * PAIR)
        score = dot(kb[rows, ls], q[cols, ls], ((1,), (1,))) * (scale * LOG2E) + tab[h]
        outside = max(0, HALO - p * PAIR)
        if outside:
            score = jnp.concatenate([score[:outside] + neg, score[outside:]], axis=0)
        top = jnp.max(score, axis=0, keepdims=True)
        expo = jnp.exp2(score - top)
        prob = expo / jnp.sum(expo, axis=0, keepdims=True)
        pgrad = dot(vb[rows, ls], g[cols, ls], ((1,), (1,)))
        delta = jnp.sum(prob * pgrad, axis=0, keepdims=True)
        sgrad = prob * (pgrad - delta)
        pt[h, rows, cols] = prob.astype(BF16)
        st[h, rows, cols] = (sgrad * scale).astype(BF16)
        if first:
            acc[h] = sgrad
        else:
            acc[h] += sgrad

    def key_side(h, kblock, terms, other):
        p0, p1 = max(0, kblock - 2), min(pairs - 1, kblock)
        span = slice(p0 * PAIR, (p1 + 1) * PAIR)
        rows = slice(kblock * PAIR, (kblock + 1) * PAIR)
        return dot(terms[h, rows, span], other[span, lanes_of(h)], ((1,), (0,)))

    def bias_row(h):
        total = jnp.sum(acc[h, 0:PAIR], axis=0, keepdims=True)
        far = pltpu.roll(diagonal_sums(acc[h, PAIR : 2 * PAIR]), 191, 1)
        near = pltpu.roll(diagonal_sums(acc[h, 2 * PAIR : SPAN]), 63, 1)
        inner = (lane >= SEG) & (lane < BUCKETS)
        rest = jnp.where(inner, 0.0, far) + jnp.concatenate([total, jnp.zeros_like(total)], axis=1)
        rest = jnp.sum(rest, axis=1, keepdims=True)
        out = jnp.where(lane < BUCKETS, near, 0.0) + jnp.where(inner, far, 0.0)
        return out + jnp.where(lane == BUCKETS - 1, rest, 0.0)

    def give_back(h):
        ls = lanes_of(h)
        for kblock in range(HALO // PAIR):
            rows = slice(kblock * PAIR, (kblock + 1) * PAIR)
            out_k[rows, ls] = key_side(h, kblock, st, q).astype(BF16)
            out_v[rows, ls] = key_side(h, kblock, pt, g).astype(BF16)
        lane_ds = pl.ds(h * HEAD_DIM, HEAD_DIM)
        return [
            send(o.at[:, lane_ds], i.at[:, lane_ds], back_send.at[2 * h + n], back_recv.at[2 * h + n], {"sp": prv})
            for n, (o, i) in enumerate(((out_k, in_k), (out_v, in_v)))
        ]

    for h in range(heads):
        block(h, pairs - 1, True)
    back = []
    for h in range(heads):
        for p in range(pairs - 2, -1, -1):
            for a in range(2):
                halo[h, a, p].wait_recv()
            block(h, p, False)
        row = bias_row(h)
        by[yi, 2 * h : 2 * h + 1, :] = row[:, :PAIR]
        by[yi, 2 * h + 1 : 2 * h + 2, :] = row[:, PAIR:]
        if h < heads - 1:
            back += give_back(h)

    rows = 2 * heads

    def spread(buf, me, peers, axis, ssem, rsem):
        for i, peer in enumerate(peers):
            send(buf.at[me, pl.ds(0, rows)], buf.at[me, pl.ds(0, rows)], ssem.at[i], rsem.at[me], {axis: peer})

    def gathered(buf, me, count, axis, ssem, rsem):
        for i in range(1, count):
            slot = lax.rem(me + i, count)
            pltpu.make_async_remote_copy(
                src_ref=buf.at[slot, pl.ds(0, rows)], dst_ref=buf.at[slot, pl.ds(0, rows)],
                send_sem=ssem.at[0], recv_sem=rsem.at[slot],
                device_id={axis: 0}, device_id_type=MESH,
            ).wait_recv()

    spread(by, yi, y_peers, "sp", y_send, y_recv)
    back += give_back(heads - 1)

    own = tokens // PAIR
    late = HALO // PAIR
    for h in range(heads):
        ls = lanes_of(h)
        for p in range(pairs):
            rows_p = slice(p * PAIR, p * PAIR + SPAN)
            cols = slice(p * PAIR, (p + 1) * PAIR)
            dq_ref[0, cols, ls] = dot(st[h, rows_p, cols], kb[rows_p, ls], ((0,), (0,))).astype(BF16)
        for n in range(own - late):
            rows_n = slice(n * PAIR, (n + 1) * PAIR)
            dk_ref[0, rows_n, ls] = key_side(h, late + n, st, q).astype(BF16)
            dv_ref[0, rows_n, ls] = key_side(h, late + n, pt, g).astype(BF16)

    gathered(by, yi, RING, "sp", y_send, y_recv)
    total = by[0, 0:rows]
    for i in range(1, RING):
        total += by[i, 0:rows]
    bz[zi, 0:rows] = total
    spread(bz, zi, z_peers, "sp", z_send, z_recv)

    for h in range(heads):
        ls = lanes_of(h)
        for cp in back[2 * h : 2 * h + 2]:
            cp.wait_recv()
        for n in range(own - late, own):
            rows_n = slice(n * PAIR, (n + 1) * PAIR)
            rows_i = slice((n - own + late) * PAIR, (n - own + late + 1) * PAIR)
            dk_ref[0, rows_n, ls] = (key_side(h, late + n, st, q) + in_k[rows_i, ls].astype(F32)).astype(BF16)
            dv_ref[0, rows_n, ls] = (key_side(h, late + n, pt, g) + in_v[rows_i, ls].astype(F32)).astype(BF16)

    gathered(bz, zi, zs, "sp", z_send, z_recv)
    total = bz[0, 0:rows]
    for i in range(1, zs):
        total += bz[i, 0:rows]
    bt[tp, 0:rows] = total
    spread(bt, tp, t_peers, "tp", t_send, t_recv)
    gathered(bt, tp, tps, "tp", t_send, t_recv)
    for t in range(tps):
        for h in range(heads):
            r = t * heads + h
            db_ref[r : r + 1, :PAIR] = bt[t, 2 * h : 2 * h + 1, :]
            db_ref[r : r + 1, PAIR:] = bt[t, 2 * h + 1 : 2 * h + 2, : BUCKETS - PAIR]
    for cp in sent:
        cp.wait_send()


def local(queries, keys, values, rel_bias, out_grad):
    _, tokens, width = queries.shape
    heads = width // HEAD_DIM
    tps = lax.axis_size("tp")
    zs = lax.axis_size("sp") // RING
    band = tokens + HALO
    dma = pltpu.SemaphoreType.DMA
    grad = jax.ShapeDtypeStruct(queries.shape, BF16)
    anywhere = pl.BlockSpec(memory_space=pl.ANY)
    vmem = pl.BlockSpec(memory_space=pltpu.VMEM)
    return pl.pallas_call(
        functools.partial(body, tokens, heads),
        out_shape=(grad, grad, grad, jax.ShapeDtypeStruct((heads * tps, BUCKETS), F32)),
        in_specs=[anywhere, anywhere, anywhere, vmem, anywhere],
        out_specs=(vmem, vmem, vmem, vmem),
        scratch_shapes=[
            pltpu.VMEM((tokens, width), BF16),
            pltpu.VMEM((tokens, width), BF16),
            pltpu.VMEM((band, width), BF16),
            pltpu.VMEM((band, width), BF16),
            pltpu.VMEM((heads, band, tokens), BF16),
            pltpu.VMEM((heads, band, tokens), BF16),
            pltpu.VMEM((heads, SPAN, PAIR), F32),
            pltpu.VMEM((heads, SPAN, PAIR), F32),
            pltpu.VMEM((8, 2 * PAIR), F32),
            pltpu.VMEM((HALO, width), BF16),
            pltpu.VMEM((HALO, width), BF16),
            pltpu.VMEM((HALO, width), BF16),
            pltpu.VMEM((HALO, width), BF16),
            pltpu.VMEM((RING, 8, PAIR), F32),
            pltpu.VMEM((zs, 8, PAIR), F32),
            pltpu.VMEM((tps, 8, PAIR), F32),
            dma((6,)),
            dma((4 * heads,)),
            dma((4 * heads,)),
            dma((2 * heads,)),
            dma((2 * heads,)),
            dma((RING,)),
            dma((RING,)),
            dma((zs,)),
            dma((zs,)),
            dma((tps,)),
            dma((tps,)),
        ],
        compiler_params=pltpu.CompilerParams(collective_id=0, has_side_effects=True),
    )(queries, keys, values, rel_bias, out_grad)


def solution(mesh):
    return jax.shard_map(
        local,
        mesh=mesh,
        in_specs=(
            P(None, "sp", "tp"),
            P(None, "sp", "tp"),
            P(None, "sp", "tp"),
            P("tp", None),
            P(None, "sp", "tp"),
        ),
        out_specs=(P(None, "sp", "tp"), P(None, "sp", "tp"), P(None, "sp", "tp"), P()),
        check_vma=False,
    )
```

time: 84.8 us -> 42.8 us (0.50)
  Pallas kernels: 0 us -> 37.7 us
  starting transfers between devices: 34.8 us -> 0 us
  local copies, waits for them, and re-layouts: 20.8 us -> 3.98 us
  matrix products: 12.3 us -> 0 us
  waiting for transfers between devices: 10.3 us -> 0 us
  other arithmetic: 4.67 us -> 0 us
    pallas_call x0 -> x1, Pallas kernels: none -> 37.7 us  [local(): pl.pallas_call(functools.partial(body, tokens, heads), out_shape=(grad, g...]
    all_to_all x2 -> x0, starting transfers between devices: 24.8 us -> none  [copy_for_each(): return lax.all_to_all(copies, axis, split_axis=0, concat_axis=0, tiled=True)]
    dot_general x27 -> x0, matrix products: 12.3 us -> none  [the longest x5 4.16 us: band_core(): jnp.einsum('sncha,snkha->snhck', g_segs, v_band[:, offset:offset + seg_co...]
    all_to_all x2 -> x0, waiting for transfers between devices: 10.3 us -> none  [copy_for_each(): return lax.all_to_all(copies, axis, split_axis=0, concat_axis=0, tiled=True)]
    ppermute x4 -> x0, starting transfers between devices: 9.92 us -> none  [from_behind(): lax.ppermute(value, axis, [(source, source + steps) for source in range(l...]
    slice x9 -> x0, local copies, waits for them, and re-layouts: 6.16 us -> none  [the longest x1 0.92 us: local(): keys[:, tok_rows - reach:]]
    concatenate x5 -> x0, local copies, waits for them, and re-layouts: 4.58 us -> none  [the longest x1 1.71 us: band_core(): prob_grad = jnp.concatenate(prob_parts, axis=-1)]
    reduce_sum x5 -> x0, other arithmetic: 2.53 us -> none  [the longest x1 1.35 us: band_core(): bias_terms = jnp.sum(score_grad, axis=(0, 1))]
  transfers between devices with their start and end apart: 6 -> 0, of which waited for: 2 -> 0; matrix products, arithmetic and copies ran while one was open for 20% -> 0% of each run, Pallas kernels for 0% -> 0%
where the time goes in v1:
time: 42.8 us; the launch traced here: 42.3 us
  Pallas kernels  37.7 us (88%)
  local copies, waits for them, and re-layouts  3.98 us (9%)
  between operations  0.65 us (2%)
    pallas_call x1, Pallas kernels, local(): pl.pallas_call(functools.partial(body, tokens, heads), out_shape=(grad, g...  37.7 us
    unnamed x10, local copies, waits for them, and re-layouts  3.98 us

profile of v1, /device:TPU:1, one launch (start us, length us, event | category | flops | bytes accessed | tf_op | source)
XLA Modules:
  0.0 42.3 jit_solution(12191870254625805825)
XLA Ops:
  0.6 37.7 %shard_map.84 = (bf16[1,384,256]{2,1,0:T(8,128)(2,1)}, bf16[1,384,256]{2,1,0:T(8,128)(2,1)}, bf16[1,384,256]{2,1,0:T(8,128)(2,1)}, f32[16,192]{1,0:T(8,128)}) custom-call(bf16[1,384,256]{2,1,0:T(8,128)(2,1)} %q_hbm.1, bf16[1,384,256]{2,1,0:T(8,128)(2,1)} %k_hbm.1, bf16[1,384,256]{2,1,0:T(8,128)(2,1)} %v_hbm.1, f32[2,192]{1,0:T(2,128)} %rb_ref.1, ...), custom_call_target="tpu_custom_call" | custom-call | tf_op jit(solution)/shard_map/pallas_call | solution.py:270
  38.3 0.0 copy-start.1
  38.3 1.7 %copy.13 = bf16[1,384,256]{2,1,0:T(8,128)(2,1)} copy(bf16[1,384,256]{2,1,0:T(8,128)(2,1)} %get-tuple-element.8) | data formatting | bytes 393216
  40.0 0.0 copy-done.1
  40.0 0.0 copy-start
  40.0 0.7 %copy.14 = bf16[1,384,256]{2,1,0:T(8,128)(2,1)} copy(bf16[1,384,256]{2,1,0:T(8,128)(2,1)S(1)} %copy-done.1) | data formatting | bytes 393216
  40.7 0.3 copy-done
  41.0 0.0 copy-start.2
  41.0 0.7 %copy.15 = bf16[1,384,256]{2,1,0:T(8,128)(2,1)} copy(bf16[1,384,256]{2,1,0:T(8,128)(2,1)S(1)} %copy-done) | data formatting | bytes 393216
  41.7 0.0 copy-done.2
  41.7 0.6 %copy.16 = f32[16,192]{1,0:T(8,128)} copy(f32[16,192]{1,0:T(8,128)S(1)} %copy-done.2) | data formatting | bytes 24576
Async XLA Ops:
  38.3 1.7 %copy-start.1 = (bf16[1,384,256]{2,1,0:T(8,128)(2,1)S(1)}, bf16[1,384,256]{2,1,0:T(8,128)(2,1)}, u32[]{:S(2)}) copy-start(bf16[1,384,256]{2,1,0:T(8,128)(2,1)} %get-tuple-element.9) | copy-start | bytes 589828
  40.0 1.0 %copy-start = (bf16[1,384,256]{2,1,0:T(8,128)(2,1)S(1)}, bf16[1,384,256]{2,1,0:T(8,128)(2,1)}, u32[]{:S(2)}) copy-start(bf16[1,384,256]{2,1,0:T(8,128)(2,1)} %get-tuple-element.10) | copy-start | bytes 589828
  41.0 0.7 %copy-start.2 = (f32[16,192]{1,0:T(8,128)S(1)}, f32[16,192]{1,0:T(8,128)}, u32[]{:S(2)}) copy-start(f32[16,192]{1,0:T(8,128)} %get-tuple-element.11) | copy-start | bytes 36868

commit v2 on v1

--- a/solution.py
+++ b/solution.py
@@ -257,6 +257,15 @@
         cp.wait_send()
 
 
+def put_out(*refs):
+    ins, outs, sem = refs[:4], refs[4:8], refs[8]
+    copies = [pltpu.make_async_copy(i, o, sem.at[n]) for n, (i, o) in enumerate(zip(ins, outs))]
+    for cp in copies:
+        cp.start()
+    for cp in copies:
+        cp.wait()
+
+
 def local(queries, keys, values, rel_bias, out_grad):
     _, tokens, width = queries.shape
     heads = width // HEAD_DIM
@@ -267,9 +276,11 @@
     grad = jax.ShapeDtypeStruct(queries.shape, BF16)
     anywhere = pl.BlockSpec(memory_space=pl.ANY)
     vmem = pl.BlockSpec(memory_space=pltpu.VMEM)
-    return pl.pallas_call(
+    bias = jax.ShapeDtypeStruct((heads * tps, BUCKETS), F32)
+    outs = (grad, grad, grad, bias)
+    held = pl.pallas_call(
         functools.partial(body, tokens, heads),
-        out_shape=(grad, grad, grad, jax.ShapeDtypeStruct((heads * tps, BUCKETS), F32)),
+        out_shape=tuple(pltpu.VMEM(o.shape, o.dtype) for o in outs),
         in_specs=[anywhere, anywhere, anywhere, vmem, anywhere],
         out_specs=(vmem, vmem, vmem, vmem),
         scratch_shapes=[
@@ -303,6 +314,13 @@
         ],
         compiler_params=pltpu.CompilerParams(collective_id=0, has_side_effects=True),
     )(queries, keys, values, rel_bias, out_grad)
+    return pl.pallas_call(
+        put_out,
+        out_shape=outs,
+        in_specs=[vmem] * 4,
+        out_specs=(anywhere,) * 4,
+        scratch_shapes=[dma((4,))],
+    )(*[pltpu.with_memory_space_constraint(x, pltpu.VMEM) for x in held])
 
 
 def solution(mesh):

time: 42.8 us -> 38.7 us (0.904)
  local copies, waits for them, and re-layouts: 3.98 us -> 0 us
    unnamed x10 -> x0, local copies, waits for them, and re-layouts: 3.98 us -> none
    pallas_call x1 -> x2, Pallas kernels: 37.7 us -> 37.7 us  [the longest x1 36.8 us: local(): pl.pallas_call(functools.partial(body, tokens, heads), out_shape=tuple((p...]
where the time goes in v2:
time: 38.7 us; the launch traced here: 38.3 us
  Pallas kernels  37.7 us (97%)
  between operations  0.64 us (2%)
    pallas_call x1, Pallas kernels, local(): pl.pallas_call(functools.partial(body, tokens, heads), out_shape=tuple((p...  36.8 us
    pallas_call x1, Pallas kernels, local(): pl.pallas_call(put_out, out_shape=outs, in_specs=[vmem] * 4, out_specs=(a...  0.85 us

profile of v2, /device:TPU:1, one launch (start us, length us, event | category | flops | bytes accessed | tf_op | source)
XLA Modules:
  0.0 38.3 jit_solution(87496212765080273)
XLA Ops:
  0.6 36.8 %shard_map.84 = (bf16[1,384,256]{2,1,0:T(8,128)(2,1)S(1)}, bf16[1,384,256]{2,1,0:T(8,128)(2,1)S(1)}, bf16[1,384,256]{2,1,0:T(8,128)(2,1)S(1)}, f32[16,192]{1,0:T(8,128)S(1)}) custom-call(bf16[1,384,256]{2,1,0:T(8,128)(2,1)} %q_hbm.1, bf16[1,384,256]{2,1,0:T(8,128)(2,1)} %k_hbm.1, bf16[1,384,256]{2,1,0:T(8,128)(2,1)} %v_hbm.1, f32[2,192]{1,0:T(2,128)} %rb_ref.1, ...), custom_call_target="tpu_custom_call" | custom-call | tf_op jit(solution)/shard_map/pallas_call | solution.py:281
  37.5 0.8 %shard_map.85 = (bf16[1,384,256]{2,1,0:T(8,128)(2,1)}, bf16[1,384,256]{2,1,0:T(8,128)(2,1)}, bf16[1,384,256]{2,1,0:T(8,128)(2,1)}, f32[16,192]{1,0:T(8,128)}) custom-call(bf16[1,384,256]{2,1,0:T(8,128)(2,1)S(1)} %get-tuple-element.8.refs_0_, bf16[1,384,256]{2,1,0:T(8,128)(2,1)S(1)} %get-tuple-element.9.refs_1_, ...), custom_call_target="tpu_custom_call" | custom-call | tf_op jit(solution)/shard_map/pallas_call | solution.py:317

commit v3 on v2

--- a/solution.py
+++ b/solution.py
@@ -1,4 +1,5 @@
 import functools
+import itertools
 
 import jax
 import jax.numpy as jnp
@@ -30,22 +31,26 @@
     return slice(head * HEAD_DIM, (head + 1) * HEAD_DIM)
 
 
-def diagonal_sums(block):
+def diagonal_sums(block, offset):
     x = jnp.concatenate([block, jnp.zeros_like(block)], axis=1)
-    rows = x.shape[0]
-    while rows > 1:
-        rows //= 2
-        x = x[:rows] + pltpu.roll(x[rows:], 2 * PAIR - rows, 1)
-    return x
+    span = 2 * PAIR
+    eight = jnp.zeros((8, span), F32)
+    for r in range(0, x.shape[0], 8):
+        eight += pltpu.roll(x[r : r + 8], (offset - r) % span, 1)
+    row = lax.broadcasted_iota(jnp.int32, (8, span), 0)
+    out = jnp.where(row == 0, eight, 0.0)
+    for r in range(1, 8):
+        out += jnp.where(row == r, pltpu.roll(eight, span - r, 1), 0.0)
+    return jnp.sum(out, axis=0, keepdims=True)
 
 
 def body(
     tokens, heads, q_hbm, k_hbm, v_hbm, rb_ref, g_hbm,
     dq_ref, dk_ref, dv_ref, db_ref,
     q, g, kb, vb, pt, st, tab, acc, rbs,
-    out_k, out_v, in_k, in_v, by, bz, bt,
+    out_k, out_v, in_k, in_v, by, bz, round_sem,
     load_sem, halo_send, halo_recv, back_send, back_recv,
-    y_send, y_recv, z_send, z_recv, t_send, t_recv,
+    y_send, y_recv, z_send, z_recv,
 ):
     sp = lax.axis_index("sp")
     tp = lax.axis_index("tp")
@@ -74,15 +79,28 @@
     q_all = load(q_hbm.at[0], q)
     g_all = load(g_hbm.at[0], g)
 
-    y_peers = [zi * RING + lax.rem(yi + i, RING) for i in range(1, RING)]
-    z_peers = [lax.rem(zi + i, zs) * RING + yi for i in range(1, zs)]
-    t_peers = [lax.rem(tp + i, tps) for i in range(1, tps)]
+    sizes = {"z": zs, "y": RING, "x": tps // 2, "c": 2}
+    here = {"z": zi, "y": yi, "x": lax.div(tp, 2), "c": lax.rem(tp, 2)}
+
+    def at(**moves):
+        c = {a: lax.rem(here[a] + moves[a], sizes[a]) if a in moves else here[a] for a in sizes}
+        return {"sp": c["z"] * RING + c["y"], "tp": c["x"] * 2 + c["c"]}
+
+    def steps(reach, axes):
+        return [(a, m) for a in axes for m in sorted({r % sizes[a] for r in reach} - {0})]
+
+    def greet(sem, moves, extra=()):
+        for where in [at(**{a: m}) for a, m in moves] + list(extra):
+            pl.semaphore_signal(sem, inc=1, device_id=where, device_id_type=MESH)
+        return len(moves) + len(extra)
+
+    def hear(sem, count):
+        if count:
+            pl.semaphore_wait(sem, count)
+
+    near = steps((1, -1), "zyxc")
     barrier = pltpu.get_barrier_semaphore()
-    for peer in [nxt, prv] + y_peers + z_peers:
-        pl.semaphore_signal(barrier, inc=1, device_id={"sp": peer}, device_id_type=MESH)
-    for peer in t_peers:
-        pl.semaphore_signal(barrier, inc=1, device_id={"tp": peer}, device_id_type=MESH)
-    pl.semaphore_wait(barrier, 2 + len(y_peers) + len(z_peers) + len(t_peers))
+    pl.semaphore_wait(barrier, greet(barrier, near, [{"sp": nxt}, {"sp": prv}]))
 
     sent = []
 
@@ -107,6 +125,8 @@
                     band.at[pl.ds(part * PAIR, PAIR), pl.ds(h * HEAD_DIM, HEAD_DIM)],
                     halo_send.at[n], halo_recv.at[n], {"sp": nxt},
                 )
+
+    heard = greet(round_sem.at[0], near)
 
     scale = HEAD_DIM ** (-0.5)
     neg = jnp.where(sp == 0, F32(NEG), F32(0.0))
@@ -158,14 +178,16 @@
         return dot(terms[h, rows, span], other[span, lanes_of(h)], ((1,), (0,)))
 
     def bias_row(h):
+        base = SEG * h
         total = jnp.sum(acc[h, 0:PAIR], axis=0, keepdims=True)
-        far = pltpu.roll(diagonal_sums(acc[h, PAIR : 2 * PAIR]), 191, 1)
-        near = pltpu.roll(diagonal_sums(acc[h, 2 * PAIR : SPAN]), 63, 1)
-        inner = (lane >= SEG) & (lane < BUCKETS)
+        far = diagonal_sums(acc[h, PAIR : 2 * PAIR], 191 + base)
+        near = diagonal_sums(acc[h, 2 * PAIR : SPAN], 63 + base)
+        place = lane - base
+        inner = (place >= SEG) & (place < BUCKETS)
         rest = jnp.where(inner, 0.0, far) + jnp.concatenate([total, jnp.zeros_like(total)], axis=1)
         rest = jnp.sum(rest, axis=1, keepdims=True)
-        out = jnp.where(lane < BUCKETS, near, 0.0) + jnp.where(inner, far, 0.0)
-        return out + jnp.where(lane == BUCKETS - 1, rest, 0.0)
+        out = jnp.where((place >= 0) & (place < BUCKETS), near, 0.0) + jnp.where(inner, far, 0.0)
+        return out + jnp.where(place == BUCKETS - 1, rest, 0.0)
 
     def give_back(h):
         ls = lanes_of(h)
@@ -181,34 +203,54 @@
 
     for h in range(heads):
         block(h, pairs - 1, True)
+    hear(round_sem.at[0], heard)
+    heard = greet(round_sem.at[1], steps((2, -2), "zy"))
     back = []
+    rows_of = []
     for h in range(heads):
         for p in range(pairs - 2, -1, -1):
             for a in range(2):
                 halo[h, a, p].wait_recv()
             block(h, p, False)
-        row = bias_row(h)
-        by[yi, 2 * h : 2 * h + 1, :] = row[:, :PAIR]
-        by[yi, 2 * h + 1 : 2 * h + 2, :] = row[:, PAIR:]
-        if h < heads - 1:
+        rows_of.append(bias_row(h))
+        if h == 0:
+            hear(round_sem.at[1], heard)
+            heard = greet(round_sem.at[2], steps((1, 2, 3), "xc"))
             back += give_back(h)
-
-    rows = 2 * heads
-
-    def spread(buf, me, peers, axis, ssem, rsem):
-        for i, peer in enumerate(peers):
-            send(buf.at[me, pl.ds(0, rows)], buf.at[me, pl.ds(0, rows)], ssem.at[i], rsem.at[me], {axis: peer})
-
-    def gathered(buf, me, count, axis, ssem, rsem):
-        for i in range(1, count):
-            slot = lax.rem(me + i, count)
-            pltpu.make_async_remote_copy(
-                src_ref=buf.at[slot, pl.ds(0, rows)], dst_ref=buf.at[slot, pl.ds(0, rows)],
-                send_sem=ssem.at[0], recv_sem=rsem.at[slot],
-                device_id={axis: 0}, device_id_type=MESH,
-            ).wait_recv()
-
-    spread(by, yi, y_peers, "sp", y_send, y_recv)
+    hear(round_sem.at[2], heard)
+
+    def spread(buf, axes, rows, ssem, rsem, values):
+        moves = [m for m in itertools.product(*(range(sizes[a]) for a in axes)) if any(m)]
+        moves.sort(key=lambda m: -sum(min(v, sizes[a] - v) for a, v in zip(axes, m)))
+
+        def slot(m):
+            n = 0
+            for a, v in zip(axes, m):
+                n = n * sizes[a] + lax.rem(here[a] + v, sizes[a])
+            return n
+
+        mine = slot((0,) * len(axes))
+        for r, value in enumerate(values):
+            buf[mine, r : r + 1, :] = value
+        part = pl.ds(0, rows)
+        for n, m in enumerate(moves):
+            send(buf.at[mine, part], buf.at[mine, part], ssem.at[n], rsem.at[mine], at(**dict(zip(axes, m))))
+
+        def collect():
+            for m in reversed(moves):
+                other = buf.at[slot(m), part]
+                pltpu.make_async_remote_copy(
+                    src_ref=other, dst_ref=other, send_sem=ssem.at[0], recv_sem=rsem.at[slot(m)],
+                    device_id=at(), device_id_type=MESH,
+                ).wait_recv()
+
+        return collect
+
+    first, second = rows_of
+    collect = spread(
+        bz, "zc", 3, z_send, z_recv,
+        [first[:, :PAIR], first[:, PAIR:] + second[:, :PAIR], second[:, PAIR:]],
+    )
     back += give_back(heads - 1)
 
     own = tokens // PAIR
@@ -224,12 +266,14 @@
             dk_ref[0, rows_n, ls] = key_side(h, late + n, st, q).astype(BF16)
             dv_ref[0, rows_n, ls] = key_side(h, late + n, pt, g).astype(BF16)
 
-    gathered(by, yi, RING, "sp", y_send, y_recv)
-    total = by[0, 0:rows]
-    for i in range(1, RING):
-        total += by[i, 0:rows]
-    bz[zi, 0:rows] = total
-    spread(bz, zi, z_peers, "sp", z_send, z_recv)
+    collect()
+    values = []
+    for c in range(2):
+        total = bz[c, 0:3]
+        for z in range(1, zs):
+            total += bz[2 * z + c, 0:3]
+        values += [total[r : r + 1] for r in range(3)]
+    collect = spread(by, "yx", 6, y_send, y_recv, values)
 
     for h in range(heads):
         ls = lanes_of(h)
@@ -241,18 +285,20 @@
             dk_ref[0, rows_n, ls] = (key_side(h, late + n, st, q) + in_k[rows_i, ls].astype(F32)).astype(BF16)
             dv_ref[0, rows_n, ls] = (key_side(h, late + n, pt, g) + in_v[rows_i, ls].astype(F32)).astype(BF16)
 
-    gathered(bz, zi, zs, "sp", z_send, z_recv)
-    total = bz[0, 0:rows]
-    for i in range(1, zs):
-        total += bz[i, 0:rows]
-    bt[tp, 0:rows] = total
-    spread(bt, tp, t_peers, "tp", t_send, t_recv)
-    gathered(bt, tp, tps, "tp", t_send, t_recv)
-    for t in range(tps):
-        for h in range(heads):
-            r = t * heads + h
-            db_ref[r : r + 1, :PAIR] = bt[t, 2 * h : 2 * h + 1, :]
-            db_ref[r : r + 1, PAIR:] = bt[t, 2 * h + 1 : 2 * h + 2, : BUCKETS - PAIR]
+    collect()
+    xs = tps // 2
+    for x in range(xs):
+        total = by[x, 0:6]
+        for y in range(1, RING):
+            total += by[y * xs + x, 0:6]
+        for c in range(2):
+            r = 2 * (2 * x + c)
+            low, mid, high = (total[3 * c + n : 3 * c + n + 1] for n in range(3))
+            db_ref[r : r + 1, :PAIR] = low
+            db_ref[r : r + 1, PAIR:] = mid[:, : BUCKETS - PAIR]
+            both = pltpu.roll(jnp.concatenate([mid, high], axis=1), 2 * PAIR - SEG, 1)
+            db_ref[r + 1 : r + 2, :PAIR] = both[:, :PAIR]
+            db_ref[r + 1 : r + 2, PAIR:] = both[:, PAIR:BUCKETS]
     for cp in sent:
         cp.wait_send()
 
@@ -297,20 +343,18 @@
             pltpu.VMEM((HALO, width), BF16),
             pltpu.VMEM((HALO, width), BF16),
             pltpu.VMEM((HALO, width), BF16),
-            pltpu.VMEM((RING, 8, PAIR), F32),
-            pltpu.VMEM((zs, 8, PAIR), F32),
-            pltpu.VMEM((tps, 8, PAIR), F32),
+            pltpu.VMEM((RING * tps // 2, 8, PAIR), F32),
+            pltpu.VMEM((zs * 2, 8, PAIR), F32),
+            pltpu.SemaphoreType.REGULAR((3,)),
             dma((6,)),
             dma((4 * heads,)),
             dma((4 * heads,)),
             dma((2 * heads,)),
             dma((2 * heads,)),
-            dma((RING,)),
-            dma((RING,)),
-            dma((zs,)),
-            dma((zs,)),
-            dma((tps,)),
-            dma((tps,)),
+            dma((RING * tps // 2,)),
+            dma((RING * tps // 2,)),
+            dma((zs * 2,)),
+            dma((zs * 2,)),
         ],
         compiler_params=pltpu.CompilerParams(collective_id=0, has_side_effects=True),
     )(queries, keys, values, rel_bias, out_grad)

time: 38.7 us -> 35.1 us (0.907)
  Pallas kernels: 37.7 us -> 34.3 us
    pallas_call x1, Pallas kernels: 36.8 us -> 33.4 us  [local(): pl.pallas_call(functools.partial(body, tokens, heads), out_shape=tuple((p...]
where the time goes in v3:
time: 35.1 us; the launch traced here: 34.9 us
  Pallas kernels  34.3 us (98%)
  between operations  0.64 us (2%)
    pallas_call x1, Pallas kernels, local(): pl.pallas_call(functools.partial(body, tokens, heads), out_shape=tuple((p...  33.4 us
    pallas_call x1, Pallas kernels, local(): pl.pallas_call(put_out, out_shape=outs, in_specs=[vmem] * 4, out_specs=(a...  0.85 us

profile of v3, /device:TPU:1, one launch (start us, length us, event | category | flops | bytes accessed | tf_op | source)
XLA Modules:
  0.0 34.9 jit_solution(17901897624719785086)
XLA Ops:
  0.6 33.4 %shard_map.84 = (bf16[1,384,256]{2,1,0:T(8,128)(2,1)S(1)}, bf16[1,384,256]{2,1,0:T(8,128)(2,1)S(1)}, bf16[1,384,256]{2,1,0:T(8,128)(2,1)S(1)}, f32[16,192]{1,0:T(8,128)S(1)}) custom-call(bf16[1,384,256]{2,1,0:T(8,128)(2,1)} %q_hbm.1, bf16[1,384,256]{2,1,0:T(8,128)(2,1)} %k_hbm.1, bf16[1,384,256]{2,1,0:T(8,128)(2,1)} %v_hbm.1, f32[2,192]{1,0:T(2,128)} %rb_ref.1, ...), custom_call_target="tpu_custom_call" | custom-call | tf_op jit(solution)/shard_map/pallas_call | solution.py:327
  34.1 0.8 %shard_map.85 = (bf16[1,384,256]{2,1,0:T(8,128)(2,1)}, bf16[1,384,256]{2,1,0:T(8,128)(2,1)}, bf16[1,384,256]{2,1,0:T(8,128)(2,1)}, f32[16,192]{1,0:T(8,128)}) custom-call(bf16[1,384,256]{2,1,0:T(8,128)(2,1)S(1)} %get-tuple-element.8.refs_0_, bf16[1,384,256]{2,1,0:T(8,128)(2,1)S(1)} %get-tuple-element.9.refs_1_, ...), custom_call_target="tpu_custom_call" | custom-call | tf_op jit(solution)/shard_map/pallas_call | solution.py:361

commit v4 on v3

--- a/solution.py
+++ b/solution.py
@@ -45,11 +45,12 @@
 
 
 def body(
-    tokens, heads, q_hbm, k_hbm, v_hbm, rb_ref, g_hbm,
+    tokens, heads, q_hbm, k_hbm, v_hbm, rb_hbm, g_hbm,
     dq_ref, dk_ref, dv_ref, db_ref,
-    q, g, kb, vb, pt, st, tab, acc, rbs,
-    out_k, out_v, in_k, in_v, by, bz, round_sem,
-    load_sem, halo_send, halo_recv, back_send, back_recv,
+    q, g, q0, g0, kb, vb, pt, st, tab, acc, rbs, rb,
+    out_k, out_v, in_k, in_v, fwd, got, part_k, part_v, by, bz, round_sem,
+    load_sem, halo_send, halo_recv, ahead_send, ahead_recv,
+    back_send, back_recv, fwd_send, fwd_recv,
     y_send, y_recv, z_send, z_recv,
 ):
     sp = lax.axis_index("sp")
@@ -63,7 +64,31 @@
     prv = lax.rem(sp + ring - 1, ring)
     pairs = tokens // PAIR
 
-    tail = tokens - HALO
+    sizes = {"z": zs, "y": RING, "x": tps // 2, "c": 2}
+    here = {"z": zi, "y": yi, "x": lax.div(tp, 2), "c": lax.rem(tp, 2)}
+
+    def at(**moves):
+        c = {a: lax.rem(here[a] + moves[a], sizes[a]) if a in moves else here[a] for a in sizes}
+        return {"sp": c["z"] * RING + c["y"], "tp": c["x"] * 2 + c["c"]}
+
+    def steps(reach, axes):
+        return [(a, m) for a in axes for m in sorted({r % sizes[a] for r in reach} - {0})]
+
+    def greet(sem, moves, extra=()):
+        for where in [at(**{a: m}) for a, m in moves] + list(extra):
+            pl.semaphore_signal(sem, inc=1, device_id=where, device_id_type=MESH)
+        return len(moves) + len(extra)
+
+    def hear(sem, count):
+        if count:
+            pl.semaphore_wait(sem, count)
+
+    near = steps((1, -1), "zyxc")
+    met = [{"sp": nxt}, {"sp": prv}] + [at(**{a: m, "c": 1}) for a, m in steps((1, -1), "z")]
+    barrier = pltpu.get_barrier_semaphore()
+    heard = greet(barrier, near, met)
+
+    before = HALO - SEG
     loads = []
 
     def load(src, dst):
@@ -72,35 +97,19 @@
         loads.append(cp)
         return cp
 
-    k_tail = load(k_hbm.at[0, pl.ds(tail, HALO)], kb.at[pl.ds(HALO + tail, HALO)])
-    v_tail = load(v_hbm.at[0, pl.ds(tail, HALO)], vb.at[pl.ds(HALO + tail, HALO)])
-    k_head = load(k_hbm.at[0, pl.ds(0, tail)], kb.at[pl.ds(HALO, tail)])
-    v_head = load(v_hbm.at[0, pl.ds(0, tail)], vb.at[pl.ds(HALO, tail)])
-    q_all = load(q_hbm.at[0], q)
-    g_all = load(g_hbm.at[0], g)
-
-    sizes = {"z": zs, "y": RING, "x": tps // 2, "c": 2}
-    here = {"z": zi, "y": yi, "x": lax.div(tp, 2), "c": lax.rem(tp, 2)}
-
-    def at(**moves):
-        c = {a: lax.rem(here[a] + moves[a], sizes[a]) if a in moves else here[a] for a in sizes}
-        return {"sp": c["z"] * RING + c["y"], "tp": c["x"] * 2 + c["c"]}
-
-    def steps(reach, axes):
-        return [(a, m) for a in axes for m in sorted({r % sizes[a] for r in reach} - {0})]
-
-    def greet(sem, moves, extra=()):
-        for where in [at(**{a: m}) for a, m in moves] + list(extra):
-            pl.semaphore_signal(sem, inc=1, device_id=where, device_id_type=MESH)
-        return len(moves) + len(extra)
-
-    def hear(sem, count):
-        if count:
-            pl.semaphore_wait(sem, count)
-
-    near = steps((1, -1), "zyxc")
-    barrier = pltpu.get_barrier_semaphore()
-    pl.semaphore_wait(barrier, greet(barrier, near, [{"sp": nxt}, {"sp": prv}]))
+    def rows_in(ref, first, count):
+        return ref.at[0, pl.ds(first, count)]
+
+    tail = tokens - before
+    k_last = load(rows_in(k_hbm, tail, before), kb.at[pl.ds(tokens, before)])
+    v_last = load(rows_in(v_hbm, tail, before), vb.at[pl.ds(tokens, before)])
+    firsts = [
+        load(rows_in(q_hbm, 0, SEG), q0),
+        load(rows_in(k_hbm, 0, SEG), kb.at[pl.ds(before, SEG)]),
+        load(rows_in(g_hbm, 0, SEG), g0),
+        load(rows_in(v_hbm, 0, SEG), vb.at[pl.ds(before, SEG)]),
+    ]
+    pl.semaphore_wait(barrier, heard)
 
     sent = []
 
@@ -113,28 +122,54 @@
         sent.append(cp)
         return cp
 
-    k_tail.wait()
-    v_tail.wait()
-    halo = {}
+    def lane_ds(h):
+        return pl.ds(h * HEAD_DIM, HEAD_DIM)
+
+    k_last.wait()
+    v_last.wait()
+    halo, ahead = {}, {}
+    cuts = ((0, PAIR), (PAIR, before - PAIR))
+    end = tokens + before
     for h in range(heads):
         for part in (1, 0):
+            first, count = cuts[part]
             for a, band in enumerate((kb, vb)):
                 n = len(halo)
                 halo[h, a, part] = send(
-                    band.at[pl.ds(tokens + part * PAIR, PAIR), pl.ds(h * HEAD_DIM, HEAD_DIM)],
-                    band.at[pl.ds(part * PAIR, PAIR), pl.ds(h * HEAD_DIM, HEAD_DIM)],
+                    band.at[pl.ds(tokens + first, count), lane_ds(h)], band.at[pl.ds(first, count), lane_ds(h)],
                     halo_send.at[n], halo_recv.at[n], {"sp": nxt},
                 )
+        if h == 0:
+            for cp in firsts:
+                cp.wait()
+        for a, (src, dst, at_src, at_dst) in enumerate(
+            ((q0, q, 0, tokens - SEG), (kb, kb, before, end), (g0, g, 0, tokens - SEG), (vb, vb, before, end))
+        ):
+            n = len(ahead)
+            ahead[h, a] = send(
+                src.at[pl.ds(at_src, SEG), lane_ds(h)], dst.at[pl.ds(at_dst, SEG), lane_ds(h)],
+                ahead_send.at[n], ahead_recv.at[n], {"sp": prv},
+            )
 
     heard = greet(round_sem.at[0], near)
+    rb_all = load(rb_hbm, rb)
+    rest = [
+        load(rows_in(q_hbm, SEG, tokens - SEG), q.at[pl.ds(0, tokens - SEG)]),
+        load(rows_in(k_hbm, SEG, tail - SEG), kb.at[pl.ds(HALO, tail - SEG)]),
+        load(rows_in(g_hbm, SEG, tokens - SEG), g.at[pl.ds(0, tokens - SEG)]),
+        load(rows_in(v_hbm, SEG, tail - SEG), vb.at[pl.ds(HALO, tail - SEG)]),
+    ]
 
     scale = HEAD_DIM ** (-0.5)
-    neg = jnp.where(sp == 0, F32(NEG), F32(0.0))
+    none_before = jnp.where(sp == 0, F32(NEG), F32(0.0))
+    none_ahead = jnp.where(sp == ring - 1, F32(NEG), F32(0.0))
+    rb_all.wait()
     rbs[...] = jnp.zeros_like(rbs)
-    rbs[0:heads, 0:BUCKETS] = rb_ref[...] * LOG2E
+    rbs[0:heads, 0:BUCKETS] = rb[...] * LOG2E
     lane = lax.broadcasted_iota(jnp.int32, (1, 2 * PAIR), 1)
     key_row = lax.broadcasted_iota(jnp.int32, (PAIR, PAIR), 0)
     q_col = lax.broadcasted_iota(jnp.int32, (PAIR, PAIR), 1)
+    q_row = lax.broadcasted_iota(jnp.int32, (1, PAIR), 1)
     for h in range(heads):
         row = rbs[h : h + 1, :]
         last = rbs[h : h + 1, BUCKETS - 1 : BUCKETS]
@@ -147,17 +182,20 @@
         tab[h, PAIR : 2 * PAIR] = far
         tab[h, 2 * PAIR : SPAN] = jnp.where((key_row >= SEG) & (q_col < SEG), NEG, near)
 
-    for cp in (k_head, v_head, q_all, g_all):
+    for cp in rest:
         cp.wait()
 
-    def block(h, p, first):
+    def block(h, p):
         ls = lanes_of(h)
         rows = slice(p * PAIR, p * PAIR + SPAN)
         cols = slice(p * PAIR, (p + 1) * PAIR)
         score = dot(kb[rows, ls], q[cols, ls], ((1,), (1,))) * (scale * LOG2E) + tab[h]
-        outside = max(0, HALO - p * PAIR)
+        outside = max(0, before - p * PAIR)
         if outside:
-            score = jnp.concatenate([score[:outside] + neg, score[outside:]], axis=0)
+            score = jnp.concatenate([score[:outside] + none_before, score[outside:]], axis=0)
+        if p == pairs - 1:
+            seen = SPAN - SEG
+            score = jnp.concatenate([score[:seen] + jnp.where(q_row >= SEG, none_ahead, 0.0), score[seen:]], axis=0)
         top = jnp.max(score, axis=0, keepdims=True)
         expo = jnp.exp2(score - top)
         prob = expo / jnp.sum(expo, axis=0, keepdims=True)
@@ -166,7 +204,7 @@
         sgrad = prob * (pgrad - delta)
         pt[h, rows, cols] = prob.astype(BF16)
         st[h, rows, cols] = (sgrad * scale).astype(BF16)
-        if first:
+        if p == pairs - 1:
             acc[h] = sgrad
         else:
             acc[h] += sgrad
@@ -189,35 +227,51 @@
         out = jnp.where((place >= 0) & (place < BUCKETS), near, 0.0) + jnp.where(inner, far, 0.0)
         return out + jnp.where(place == BUCKETS - 1, rest, 0.0)
 
+    def query_side(h, p):
+        rows = slice(p * PAIR, p * PAIR + SPAN)
+        return dot(st[h, rows, p * PAIR : (p + 1) * PAIR], kb[rows, lanes_of(h)], ((0,), (0,)))
+
     def give_back(h):
         ls = lanes_of(h)
-        for kblock in range(HALO // PAIR):
-            rows = slice(kblock * PAIR, (kblock + 1) * PAIR)
-            out_k[rows, ls] = key_side(h, kblock, st, q).astype(BF16)
-            out_v[rows, ls] = key_side(h, kblock, pt, g).astype(BF16)
-        lane_ds = pl.ds(h * HEAD_DIM, HEAD_DIM)
-        return [
-            send(o.at[:, lane_ds], i.at[:, lane_ds], back_send.at[2 * h + n], back_recv.at[2 * h + n], {"sp": prv})
-            for n, (o, i) in enumerate(((out_k, in_k), (out_v, in_v)))
+        for terms, other, out, part, m in ((st, q, out_k, part_k, 0), (pt, g, out_v, part_v, 1)):
+            out[0:PAIR, ls] = key_side(h, 0, terms, other).astype(BF16)
+            edge = key_side(h, 1, terms, other)
+            out[PAIR:before, ls] = edge[:SEG].astype(BF16)
+            part[0:SEG, ls] = edge[SEG:]
+            edge = key_side(h, 4, terms, other)
+            part[SEG:PAIR, ls] = edge[:SEG]
+            fwd[m, :, ls] = edge[SEG:].astype(BF16)
+        edge = query_side(h, pairs - 1)
+        dq_ref[0, tokens - SEG : tokens, ls] = edge[:SEG].astype(BF16)
+        fwd[2, :, ls] = edge[SEG:].astype(BF16)
+        n = 2 * h
+        pieces = [
+            send(o.at[:, lane_ds(h)], i.at[:, lane_ds(h)], back_send.at[n + a], back_recv.at[n + a], {"sp": prv})
+            for a, (o, i) in enumerate(((out_k, in_k), (out_v, in_v)))
         ]
-
-    for h in range(heads):
-        block(h, pairs - 1, True)
+        n = 3 * h
+        return pieces + [
+            send(fwd.at[a, :, lane_ds(h)], got.at[a, :, lane_ds(h)], fwd_send.at[n + a], fwd_recv.at[n + a], {"sp": nxt})
+            for a in range(3)
+        ]
+
     hear(round_sem.at[0], heard)
     heard = greet(round_sem.at[1], steps((2, -2), "zy"))
     back = []
     rows_of = []
     for h in range(heads):
+        for a in range(4):
+            ahead[h, a].wait_recv()
+        block(h, pairs - 1)
         for p in range(pairs - 2, -1, -1):
             for a in range(2):
                 halo[h, a, p].wait_recv()
-            block(h, p, False)
+            block(h, p)
         rows_of.append(bias_row(h))
         if h == 0:
-            hear(round_sem.at[1], heard)
-            heard = greet(round_sem.at[2], steps((1, 2, 3), "xc"))
             back += give_back(h)
-    hear(round_sem.at[2], heard)
+    hear(round_sem.at[1], heard)
+    heard = greet(round_sem.at[2], steps((1, 2, 3), "x"))
 
     def spread(buf, axes, rows, ssem, rsem, values):
         moves = [m for m in itertools.product(*(range(sizes[a]) for a in axes)) if any(m)]
@@ -253,18 +307,12 @@
     )
     back += give_back(heads - 1)
 
-    own = tokens // PAIR
-    late = HALO // PAIR
     for h in range(heads):
         ls = lanes_of(h)
-        for p in range(pairs):
-            rows_p = slice(p * PAIR, p * PAIR + SPAN)
-            cols = slice(p * PAIR, (p + 1) * PAIR)
-            dq_ref[0, cols, ls] = dot(st[h, rows_p, cols], kb[rows_p, ls], ((0,), (0,))).astype(BF16)
-        for n in range(own - late):
-            rows_n = slice(n * PAIR, (n + 1) * PAIR)
-            dk_ref[0, rows_n, ls] = key_side(h, late + n, st, q).astype(BF16)
-            dv_ref[0, rows_n, ls] = key_side(h, late + n, pt, g).astype(BF16)
+        for p in range(pairs - 1):
+            dq_ref[0, SEG + p * PAIR : SEG + (p + 1) * PAIR, ls] = query_side(h, p).astype(BF16)
+        for terms, other, out in ((st, q, dk_ref), (pt, g, dv_ref)):
+            out[0, SEG : SEG + PAIR, ls] = key_side(h, 2, terms, other).astype(BF16)
 
     collect()
     values = []
@@ -273,17 +321,19 @@
         for z in range(1, zs):
             total += bz[2 * z + c, 0:3]
         values += [total[r : r + 1] for r in range(3)]
+    hear(round_sem.at[2], heard)
     collect = spread(by, "yx", 6, y_send, y_recv, values)
 
     for h in range(heads):
         ls = lanes_of(h)
-        for cp in back[2 * h : 2 * h + 2]:
+        for cp in back[5 * h : 5 * h + 5]:
             cp.wait_recv()
-        for n in range(own - late, own):
-            rows_n = slice(n * PAIR, (n + 1) * PAIR)
-            rows_i = slice((n - own + late) * PAIR, (n - own + late + 1) * PAIR)
-            dk_ref[0, rows_n, ls] = (key_side(h, late + n, st, q) + in_k[rows_i, ls].astype(F32)).astype(BF16)
-            dv_ref[0, rows_n, ls] = (key_side(h, late + n, pt, g) + in_v[rows_i, ls].astype(F32)).astype(BF16)
+        dq_ref[0, 0:SEG, ls] = got[2, :, ls]
+        for terms, other, out, part, come, m in ((st, q, dk_ref, part_k, in_k, 0), (pt, g, dv_ref, part_v, in_v, 1)):
+            out[0, 0:SEG, ls] = (part[0:SEG, ls] + got[m, :, ls].astype(F32)).astype(BF16)
+            mid = key_side(h, 3, terms, other) + come[0:PAIR, ls].astype(F32)
+            out[0, tail : tail + PAIR, ls] = mid.astype(BF16)
+            out[0, tokens - SEG : tokens, ls] = (part[SEG:PAIR, ls] + come[PAIR:before, ls].astype(F32)).astype(BF16)
 
     collect()
     xs = tps // 2
@@ -327,11 +377,13 @@
     held = pl.pallas_call(
         functools.partial(body, tokens, heads),
         out_shape=tuple(pltpu.VMEM(o.shape, o.dtype) for o in outs),
-        in_specs=[anywhere, anywhere, anywhere, vmem, anywhere],
+        in_specs=[anywhere] * 5,
         out_specs=(vmem, vmem, vmem, vmem),
         scratch_shapes=[
             pltpu.VMEM((tokens, width), BF16),
             pltpu.VMEM((tokens, width), BF16),
+            pltpu.VMEM((SEG, width), BF16),
+            pltpu.VMEM((SEG, width), BF16),
             pltpu.VMEM((band, width), BF16),
             pltpu.VMEM((band, width), BF16),
             pltpu.VMEM((heads, band, tokens), BF16),
@@ -339,18 +391,27 @@
             pltpu.VMEM((heads, SPAN, PAIR), F32),
             pltpu.VMEM((heads, SPAN, PAIR), F32),
             pltpu.VMEM((8, 2 * PAIR), F32),
-            pltpu.VMEM((HALO, width), BF16),
-            pltpu.VMEM((HALO, width), BF16),
-            pltpu.VMEM((HALO, width), BF16),
-            pltpu.VMEM((HALO, width), BF16),
+            pltpu.VMEM((heads, BUCKETS), F32),
+            pltpu.VMEM((HALO - SEG, width), BF16),
+            pltpu.VMEM((HALO - SEG, width), BF16),
+            pltpu.VMEM((HALO - SEG, width), BF16),
+            pltpu.VMEM((HALO - SEG, width), BF16),
+            pltpu.VMEM((3, SEG, width), BF16),
+            pltpu.VMEM((3, SEG, width), BF16),
+            pltpu.VMEM((PAIR, width), F32),
+            pltpu.VMEM((PAIR, width), F32),
             pltpu.VMEM((RING * tps // 2, 8, PAIR), F32),
             pltpu.VMEM((zs * 2, 8, PAIR), F32),
             pltpu.SemaphoreType.REGULAR((3,)),
-            dma((6,)),
+            dma((11,)),
+            dma((4 * heads,)),
+            dma((4 * heads,)),
             dma((4 * heads,)),
             dma((4 * heads,)),
             dma((2 * heads,)),
             dma((2 * heads,)),
+            dma((3 * heads,)),
+            dma((3 * heads,)),
             dma((RING * tps // 2,)),
             dma((RING * tps // 2,)),
             dma((zs * 2,)),

time: 35.1 us -> 33.9 us (0.966)
  Pallas kernels: 34.3 us -> 33.2 us
    pallas_call x1, Pallas kernels: 33.4 us -> 32.3 us  [local(): pl.pallas_call(functools.partial(body, tokens, heads), out_shape=tuple((p...]
where the time goes in v4:
time: 33.9 us; the launch traced here: 33.8 us
  Pallas kernels  33.2 us (98%)
  between operations  0.64 us (2%)
    pallas_call x1, Pallas kernels, local(): pl.pallas_call(functools.partial(body, tokens, heads), out_shape=tuple((p...  32.3 us
    pallas_call x1, Pallas kernels, local(): pl.pallas_call(put_out, out_shape=outs, in_specs=[vmem] * 4, out_specs=(a...  0.85 us

profile of v4, /device:TPU:1, one launch (start us, length us, event | category | flops | bytes accessed | tf_op | source)
XLA Modules:
  0.0 33.8 jit_solution(5957751747926809455)
XLA Ops:
  0.6 32.3 %shard_map.84 = (bf16[1,384,256]{2,1,0:T(8,128)(2,1)S(1)}, bf16[1,384,256]{2,1,0:T(8,128)(2,1)S(1)}, bf16[1,384,256]{2,1,0:T(8,128)(2,1)S(1)}, f32[16,192]{1,0:T(8,128)S(1)}) custom-call(bf16[1,384,256]{2,1,0:T(8,128)(2,1)} %q_hbm.1, bf16[1,384,256]{2,1,0:T(8,128)(2,1)} %k_hbm.1, bf16[1,384,256]{2,1,0:T(8,128)(2,1)} %v_hbm.1, f32[2,192]{1,0:T(2,128)} %rb_hbm.1, ...), custom_call_target="tpu_custom_call" | custom-call | tf_op jit(solution)/shard_map/pallas_call | solution.py:377
  33.0 0.8 %shard_map.85 = (bf16[1,384,256]{2,1,0:T(8,128)(2,1)}, bf16[1,384,256]{2,1,0:T(8,128)(2,1)}, bf16[1,384,256]{2,1,0:T(8,128)(2,1)}, f32[16,192]{1,0:T(8,128)}) custom-call(bf16[1,384,256]{2,1,0:T(8,128)(2,1)S(1)} %get-tuple-element.8.refs_0_, bf16[1,384,256]{2,1,0:T(8,128)(2,1)S(1)} %get-tuple-element.9.refs_1_, ...), custom_call_target="tpu_custom_call" | custom-call | tf_op jit(solution)/shard_map/pallas_call | solution.py:422

commit v5 on v4

--- a/solution.py
+++ b/solution.py
@@ -31,8 +31,7 @@
     return slice(head * HEAD_DIM, (head + 1) * HEAD_DIM)
 
 
-def diagonal_sums(block, offset):
-    x = jnp.concatenate([block, jnp.zeros_like(block)], axis=1)
+def diagonal_sums(x, offset):
     span = 2 * PAIR
     eight = jnp.zeros((8, span), F32)
     for r in range(0, x.shape[0], 8):
@@ -217,15 +216,12 @@
 
     def bias_row(h):
         base = SEG * h
-        total = jnp.sum(acc[h, 0:PAIR], axis=0, keepdims=True)
-        far = diagonal_sums(acc[h, PAIR : 2 * PAIR], 191 + base)
-        near = diagonal_sums(acc[h, 2 * PAIR : SPAN], 63 + base)
-        place = lane - base
-        inner = (place >= SEG) & (place < BUCKETS)
-        rest = jnp.where(inner, 0.0, far) + jnp.concatenate([total, jnp.zeros_like(total)], axis=1)
-        rest = jnp.sum(rest, axis=1, keepdims=True)
-        out = jnp.where((place >= 0) & (place < BUCKETS), near, 0.0) + jnp.where(inner, far, 0.0)
-        return out + jnp.where(place == BUCKETS - 1, rest, 0.0)
+        far = acc[h, PAIR : 2 * PAIR]
+        clipped = key_row < q_col
+        rest = acc[h, 0:PAIR] + jnp.where(clipped, far, 0.0)
+        rest = jnp.sum(jnp.sum(rest, axis=0, keepdims=True), axis=1, keepdims=True)
+        x = jnp.concatenate([acc[h, 2 * PAIR : SPAN], jnp.where(clipped, 0.0, far)], axis=1)
+        return diagonal_sums(x, SEG - 1 + base) + jnp.where(lane == base + BUCKETS - 1, rest, 0.0)
 
     def query_side(h, p):
         rows = slice(p * PAIR, p * PAIR + SPAN)
@@ -322,6 +318,7 @@
             total += bz[2 * z + c, 0:3]
         values += [total[r : r + 1] for r in range(3)]
     hear(round_sem.at[2], heard)
+    early = len(sent)
     collect = spread(by, "yx", 6, y_send, y_recv, values)
 
     for h in range(heads):
@@ -335,6 +332,8 @@
             out[0, tail : tail + PAIR, ls] = mid.astype(BF16)
             out[0, tokens - SEG : tokens, ls] = (part[SEG:PAIR, ls] + come[PAIR:before, ls].astype(F32)).astype(BF16)
 
+    for cp in sent[:early]:
+        cp.wait_send()
     collect()
     xs = tps // 2
     for x in range(xs):
@@ -349,7 +348,7 @@
             both = pltpu.roll(jnp.concatenate([mid, high], axis=1), 2 * PAIR - SEG, 1)
             db_ref[r + 1 : r + 2, :PAIR] = both[:, :PAIR]
             db_ref[r + 1 : r + 2, PAIR:] = both[:, PAIR:BUCKETS]
-    for cp in sent:
+    for cp in sent[early:]:
         cp.wait_send()
 
 

time: 33.9 us -> 33.8 us (level)
  no operation moved by 1% of the time
where the time goes in v5:
time: 33.8 us; the launch traced here: 33.6 us
  Pallas kernels  33 us (98%)
  between operations  0.64 us (2%)
    pallas_call x1, Pallas kernels, local(): pl.pallas_call(functools.partial(body, tokens, heads), out_shape=tuple((p...  32.2 us
    pallas_call x1, Pallas kernels, local(): pl.pallas_call(put_out, out_shape=outs, in_specs=[vmem] * 4, out_specs=(a...  0.85 us

profile of v5, /device:TPU:1, one launch (start us, length us, event | category | flops | bytes accessed | tf_op | source)
XLA Modules:
  0.0 33.6 jit_solution(2714384977992566581)
XLA Ops:
  0.6 32.2 %shard_map.84 = (bf16[1,384,256]{2,1,0:T(8,128)(2,1)S(1)}, bf16[1,384,256]{2,1,0:T(8,128)(2,1)S(1)}, bf16[1,384,256]{2,1,0:T(8,128)(2,1)S(1)}, f32[16,192]{1,0:T(8,128)S(1)}) custom-call(bf16[1,384,256]{2,1,0:T(8,128)(2,1)} %q_hbm.1, bf16[1,384,256]{2,1,0:T(8,128)(2,1)} %k_hbm.1, bf16[1,384,256]{2,1,0:T(8,128)(2,1)} %v_hbm.1, f32[2,192]{1,0:T(2,128)} %rb_hbm.1, ...), custom_call_target="tpu_custom_call" | custom-call | tf_op jit(solution)/shard_map/pallas_call | solution.py:376
  32.8 0.8 %shard_map.85 = (bf16[1,384,256]{2,1,0:T(8,128)(2,1)}, bf16[1,384,256]{2,1,0:T(8,128)(2,1)}, bf16[1,384,256]{2,1,0:T(8,128)(2,1)}, f32[16,192]{1,0:T(8,128)}) custom-call(bf16[1,384,256]{2,1,0:T(8,128)(2,1)S(1)} %get-tuple-element.8.refs_0_, bf16[1,384,256]{2,1,0:T(8,128)(2,1)S(1)} %get-tuple-element.9.refs_1_, ...), custom_call_target="tpu_custom_call" | custom-call | tf_op jit(solution)/shard_map/pallas_call | solution.py:421

commit v6 on v5

--- a/solution.py
+++ b/solution.py
@@ -260,12 +260,13 @@
             ahead[h, a].wait_recv()
         block(h, pairs - 1)
         for p in range(pairs - 2, -1, -1):
+            if h and p == 0:
+                rows_of.append(bias_row(h - 1))
+                back += give_back(h - 1)
             for a in range(2):
                 halo[h, a, p].wait_recv()
             block(h, p)
-        rows_of.append(bias_row(h))
-        if h == 0:
-            back += give_back(h)
+    rows_of.append(bias_row(heads - 1))
     hear(round_sem.at[1], heard)
     heard = greet(round_sem.at[2], steps((1, 2, 3), "x"))
 

time: 33.8 us -> 33.7 us (level)
  no operation moved by 1% of the time
where the time goes in v6:
time: 33.7 us; the launch traced here: 33.5 us
  Pallas kernels  32.8 us (97%)
  between operations  0.64 us (2%)
    pallas_call x1, Pallas kernels, local(): pl.pallas_call(functools.partial(body, tokens, heads), out_shape=tuple((p...  32 us
    pallas_call x1, Pallas kernels, local(): pl.pallas_call(put_out, out_shape=outs, in_specs=[vmem] * 4, out_specs=(a...  0.85 us

profile of v6, /device:TPU:1, one launch (start us, length us, event | category | flops | bytes accessed | tf_op | source)
XLA Modules:
  0.0 33.5 jit_solution(1307913653601899031)
XLA Ops:
  0.6 32.0 %shard_map.84 = (bf16[1,384,256]{2,1,0:T(8,128)(2,1)S(1)}, bf16[1,384,256]{2,1,0:T(8,128)(2,1)S(1)}, bf16[1,384,256]{2,1,0:T(8,128)(2,1)S(1)}, f32[16,192]{1,0:T(8,128)S(1)}) custom-call(bf16[1,384,256]{2,1,0:T(8,128)(2,1)} %q_hbm.1, bf16[1,384,256]{2,1,0:T(8,128)(2,1)} %k_hbm.1, bf16[1,384,256]{2,1,0:T(8,128)(2,1)} %v_hbm.1, f32[2,192]{1,0:T(2,128)} %rb_hbm.1, ...), custom_call_target="tpu_custom_call" | custom-call | tf_op jit(solution)/shard_map/pallas_call | solution.py:377
  32.6 0.8 %shard_map.85 = (bf16[1,384,256]{2,1,0:T(8,128)(2,1)}, bf16[1,384,256]{2,1,0:T(8,128)(2,1)}, bf16[1,384,256]{2,1,0:T(8,128)(2,1)}, f32[16,192]{1,0:T(8,128)}) custom-call(bf16[1,384,256]{2,1,0:T(8,128)(2,1)S(1)} %get-tuple-element.8.refs_0_, bf16[1,384,256]{2,1,0:T(8,128)(2,1)S(1)} %get-tuple-element.9.refs_1_, ...), custom_call_target="tpu_custom_call" | custom-call | tf_op jit(solution)/shard_map/pallas_call | solution.py:422

commit v7 on v6

--- a/solution.py
+++ b/solution.py
@@ -268,7 +268,6 @@
             block(h, p)
     rows_of.append(bias_row(heads - 1))
     hear(round_sem.at[1], heard)
-    heard = greet(round_sem.at[2], steps((1, 2, 3), "x"))
 
     def spread(buf, axes, rows, ssem, rsem, values):
         moves = [m for m in itertools.product(*(range(sizes[a]) for a in axes)) if any(m)]
@@ -302,6 +301,7 @@
         bz, "zc", 3, z_send, z_recv,
         [first[:, :PAIR], first[:, PAIR:] + second[:, :PAIR], second[:, PAIR:]],
     )
+    heard = greet(round_sem.at[2], steps((1, 2, 3), "x"))
     back += give_back(heads - 1)
 
     for h in range(heads):

time: 33.7 us -> 33.7 us (level)
  no operation moved by 1% of the time
where the time goes in v7:
time: 33.7 us; the launch traced here: 33.4 us
  Pallas kernels  32.8 us (97%)
  between operations  0.64 us (2%)
    pallas_call x1, Pallas kernels, local(): pl.pallas_call(functools.partial(body, tokens, heads), out_shape=tuple((p...  32 us
    pallas_call x1, Pallas kernels, local(): pl.pallas_call(put_out, out_shape=outs, in_specs=[vmem] * 4, out_specs=(a...  0.85 us

profile of v7, /device:TPU:1, one launch (start us, length us, event | category | flops | bytes accessed | tf_op | source)
XLA Modules:
  0.0 33.4 jit_solution(2012771417697005631)
XLA Ops:
  0.6 32.0 %shard_map.84 = (bf16[1,384,256]{2,1,0:T(8,128)(2,1)S(1)}, bf16[1,384,256]{2,1,0:T(8,128)(2,1)S(1)}, bf16[1,384,256]{2,1,0:T(8,128)(2,1)S(1)}, f32[16,192]{1,0:T(8,128)S(1)}) custom-call(bf16[1,384,256]{2,1,0:T(8,128)(2,1)} %q_hbm.1, bf16[1,384,256]{2,1,0:T(8,128)(2,1)} %k_hbm.1, bf16[1,384,256]{2,1,0:T(8,128)(2,1)} %v_hbm.1, f32[2,192]{1,0:T(2,128)} %rb_hbm.1, ...), custom_call_target="tpu_custom_call" | custom-call | tf_op jit(solution)/shard_map/pallas_call | solution.py:377
  32.6 0.8 %shard_map.85 = (bf16[1,384,256]{2,1,0:T(8,128)(2,1)}, bf16[1,384,256]{2,1,0:T(8,128)(2,1)}, bf16[1,384,256]{2,1,0:T(8,128)(2,1)}, f32[16,192]{1,0:T(8,128)}) custom-call(bf16[1,384,256]{2,1,0:T(8,128)(2,1)S(1)} %get-tuple-element.8.refs_0_, bf16[1,384,256]{2,1,0:T(8,128)(2,1)S(1)} %get-tuple-element.9.refs_1_, ...), custom_call_target="tpu_custom_call" | custom-call | tf_op jit(solution)/shard_map/pallas_call | solution.py:422
